TPU v7x, 32 devices: a whole 2x2x4 slice. The times are simulated.
32 devices in a mesh: ep: 8 (over z, x), tp: 4 (over y, core).
Axes of the slice: x: 2, y: 2, z: 4, core: 2. Of those that a mesh axis runs over, the one named last changes fastest.
Arguments:
- first_batch: bfloat16 [4096, 2048], P(('ep', 'tp')), may hold values from -6 to 6
- mixer_gain: float32 [2048], replicated, may hold values from 0.1 to 1.9
- mixer_in: bfloat16 [2048, 512], P(None, 'tp'), may hold values from -0.125 to 0.125
- group_maps: bfloat16 [8, 64, 64], replicated, may hold values from -0.75 to 0.75
- pool_scale: float32 [512], replicated, may hold values from 0.1 to 1.9
- mixer_out: bfloat16 [512, 2048], P('tp'), may hold values from -0.25 to 0.25
- second_batch: bfloat16 [1024, 2048], P('ep'), may hold values from -6 to 6
- expert_gain: float32 [2048], replicated, may hold values from 0.1 to 1.9
- expert_choice: int32 [1024, 2], P('ep'), may hold values from 0 to 7, all different within a row; in each aligned block of 128 rows (0 to 127, 128 to 255, ...) at most 64 rows name the same one
- route_scores: float32 [1024, 2], P('ep'), may hold values from -6 to 6
- expert_gate: bfloat16 [8, 2048, 3584], P('ep', None, 'tp'), may hold values from -0.125 to 0.125
- expert_up: bfloat16 [8, 2048, 3584], P('ep', None, 'tp'), may hold values from -0.125 to 0.125
- expert_down: bfloat16 [8, 3584, 2048], P('ep', 'tp'), may hold values from -0.09375 to 0.09375
Outputs:
- mixed_first: bfloat16 [4096, 2048], P(('ep', 'tp'))
- experts_second: bfloat16 [1024, 2048], P('ep')
Inputs may be any that keep to these rules, and one draw needn't show every extreme that they name: `expert_choice`: the two entries of a row differ. Within the rows of one device (aligned blocks of 128 rows) no expert is named more than 64 times, a bound that some block reaches there.
All inputs are finite; a program needn't handle non-finite values.
Results may differ from a plain program's by a relative error of at most 0.018.
Values may be sent and summed in bfloat16 or wider, within the bound.
A program may use at most 64 MiB of HBM per device.

v0:
```python
import jax
import jax.numpy as jnp
from jax import lax
from jax.experimental import pallas as pl
from jax.experimental.pallas import tpu as pltpu
from jax.sharding import PartitionSpec as P

GROUP = 64
SEQS = 1


epsilon = 1e-06


def extended(block, sides, width):
    for axis, dim in sides:
        count = lax.axis_size(axis)
        forward = [(i, i + 1) for i in range(count - 1)]
        backward = [(target, source) for source, target in forward]
        low = lax.ppermute(
            lax.slice_in_dim(block, block.shape[dim] - width, None, axis=dim), axis, forward
        )
        high = lax.ppermute(lax.slice_in_dim(block, 0, width, axis=dim), axis, backward)
        block = jnp.concatenate([low, block, high], axis=dim)
    return block


def rms_scale(values, gain):
    floats = values.astype(jnp.float32)
    factor = lax.rsqrt(jnp.mean(floats * floats, axis=-1, keepdims=True) + epsilon)
    return (floats * factor * gain).astype(jnp.bfloat16)


def mixer_half(first_batch, mixer_gain, mixer_in, group_maps, pool_scale, mixer_out):
    count_rows = first_batch.shape[0]
    normed = rms_scale(first_batch, mixer_gain)
    pooled_in = jnp.dot(
        normed,
        lax.all_gather(mixer_in, "tp", axis=1, tiled=True),
        preferred_element_type=jnp.float32,
    ).astype(jnp.bfloat16)
    channels = pooled_in.shape[1]
    padded = extended(pooled_in, ((("ep", "tp"), 0),), 8).astype(jnp.float32)
    devices = lax.axis_size("ep") * lax.axis_size("tp")
    seq_length = count_rows * devices // SEQS
    first_row = (lax.axis_index("ep") * lax.axis_size("tp") + lax.axis_index("tp")) * count_rows
    places = first_row + jnp.arange(count_rows, dtype=jnp.int32)
    own_seq = places // seq_length
    group_of = jnp.arange(channels, dtype=jnp.int32) // GROUP
    half_span = jnp.left_shift(jnp.ones_like(group_of), group_of % 4)
    window_sum = jnp.zeros((count_rows, channels), jnp.float32)
    window_count = jnp.zeros((count_rows, channels), jnp.float32)
    for offset in range(-8, 8):
        inside = (
            ((places + offset) // seq_length == own_seq)[:, None]
            & (offset >= -half_span)[None, :]
            & (offset < half_span)[None, :]
        )
        window_sum = window_sum + jnp.where(
            inside, padded[8 + offset : 8 + offset + count_rows], 0.0
        )
        window_count = window_count + inside.astype(jnp.float32)
    centred = (window_sum / window_count - padded[8 : 8 + count_rows]).astype(jnp.bfloat16)
    group_count = group_maps.shape[0]
    identity = jnp.eye(group_count, dtype=jnp.bfloat16)
    block_map = jnp.einsum("gcd,gh->gchd", group_maps, identity).reshape(channels, channels)
    grouped = (jnp.dot(centred, block_map, preferred_element_type=jnp.float32) * pool_scale).astype(
        jnp.bfloat16
    )
    mixed_out = jnp.dot(
        grouped,
        lax.all_gather(mixer_out, "tp", axis=0, tiled=True),
        preferred_element_type=jnp.float32,
    )
    return mixed_out.astype(jnp.bfloat16)


def expert_half(
    second_batch, expert_gain, expert_choice, route_scores, expert_gate, expert_up, expert_down
):
    row_count = second_batch.shape[0]
    model_width = second_batch.shape[1]
    experts = lax.axis_size("ep")
    tp_count = lax.axis_size("tp")
    capacity = 4 * row_count // experts
    share = capacity // tp_count
    normed = rms_scale(second_batch, expert_gain)
    chosen = expert_choice.reshape(-1)
    one_hot = (chosen[:, None] == jnp.arange(experts, dtype=jnp.int32)[None, :]).astype(jnp.int32)
    ranking = jnp.sum(jnp.cumsum(one_hot, axis=0) * one_hot, axis=1) - 1
    slot_place = ranking * experts + chosen
    source_row = jnp.arange(chosen.shape[0], dtype=jnp.int32) // expert_choice.shape[1]
    slot_table = jnp.zeros((capacity * experts,), jnp.int32).at[slot_place].set(source_row + 1)
    outgoing = jnp.where(
        (slot_table > 0)[:, None],
        normed[jnp.maximum(slot_table - 1, 0)],
        jnp.zeros((), jnp.bfloat16),
    )
    outgoing = outgoing.reshape(capacity, experts, model_width)
    portion = lax.dynamic_slice_in_dim(outgoing, lax.axis_index("tp") * share, share, 0)
    arrived_part = lax.all_to_all(portion, "ep", split_axis=1, concat_axis=1, tiled=True)
    arrived = lax.all_gather(arrived_part, "tp", axis=0, tiled=True)
    incoming = arrived.reshape(capacity * experts, model_width)
    gate_weight = expert_gate[0]
    up_weight = expert_up[0]
    down_weight = expert_down[0]
    gate_part = jnp.dot(incoming, gate_weight, preferred_element_type=jnp.float32)
    up_part = jnp.dot(incoming, up_weight, preferred_element_type=jnp.float32)
    hidden = (jax.nn.silu(gate_part) * up_part).astype(jnp.bfloat16)
    summed = lax.psum_scatter(
        jnp.dot(hidden, down_weight, preferred_element_type=jnp.float32).astype(jnp.bfloat16),
        "tp",
        scatter_dimension=0,
        tiled=True,
    )
    finished = summed.reshape(share, experts, model_width)
    returned = lax.all_to_all(finished, "ep", split_axis=1, concat_axis=1, tiled=True)
    every_slot = lax.all_gather(returned, "tp", axis=0, tiled=True).reshape(
        capacity * experts, model_width
    )
    picked = every_slot[slot_place].reshape(row_count, -1, model_width)
    weight_first = jax.nn.sigmoid(route_scores[:, 0] - route_scores[:, 1])[:, None]
    blended = weight_first * picked[:, 0].astype(jnp.float32) + (1.0 - weight_first) * picked[
        :, 1
    ].astype(jnp.float32)
    return blended.astype(jnp.bfloat16)


MESH = pl.DeviceIdType.MESH
VMEM_LIMIT = 40 * 1024 * 1024


def greet(peers):
    barrier = pltpu.get_barrier_semaphore()
    for peer in peers:
        pl.semaphore_signal(barrier, inc=1, device_id=peer, device_id_type=MESH)
    pl.semaphore_wait(barrier, len(peers))


def places_of(count):
    row = lax.axis_index("ep")
    col = lax.axis_index("tp")
    partner = col + 1 - 2 * (col % 2)
    across = (col + 2) % 4
    others = [((row + k) % count, col) for k in range(1, count)]
    return row, col, partner, across, others


def remote(source, target, send, recv, device):
    return pltpu.make_async_remote_copy(
        src_ref=source,
        dst_ref=target,
        send_sem=send,
        recv_sem=recv,
        device_id=device,
        device_id_type=MESH,
    )


def dispatch_kernel(count, portion, result, landed, send, recv, local):
    row, col, partner, across, others = places_of(count)
    greet(others + [(row, partner), (row, across)])
    firsts = [None]
    for k in range(1, count):
        copy = remote(
            portion.at[(row + k) % count], landed.at[row, col], send.at[0, k], recv.at[0, k],
            ((row + k) % count, col),
        )
        copy.start()
        firsts.append(copy)
    own = pltpu.make_async_copy(portion.at[row], landed.at[row, col], local.at[0])
    own.start()
    own.wait()
    sides, ys, corners = [], [], []
    lag = 2
    for k in range(count + lag):
        if k < count:
            source = (row + count - k) % count
            if k > 0:
                firsts[k].wait_recv()
            block = landed.at[source, col]
            y = remote(block, block, send.at[1, k], recv.at[1, k], (row, across))
            y.start()
            side = remote(block, block, send.at[2, k], recv.at[2, k], (row, partner))
            side.start()
            ys.append(y)
            sides.append(side)
        if k >= lag:
            j = k - lag
            source = (row + count - j) % count
            ys[j].wait_recv()
            block = landed.at[source, across]
            corner = remote(block, block, send.at[3, j], recv.at[3, j], (row, partner))
            corner.start()
            corners.append(corner)
    for k in range(count):
        sides[k].wait_recv()
        corners[k].wait_recv()
    out = pltpu.make_async_copy(landed, result, local.at[1])
    out.start()
    for k in range(count):
        if k > 0:
            firsts[k].wait_send()
        ys[k].wait_send()
        sides[k].wait_send()
        corners[k].wait_send()
    out.wait()


def dispatch(portion):
    count, share, width = portion.shape
    return pl.pallas_call(
        lambda *refs: dispatch_kernel(count, *refs),
        out_shape=jax.ShapeDtypeStruct((count, 4, share, width), portion.dtype),
        in_specs=[pl.BlockSpec(memory_space=pltpu.VMEM)],
        out_specs=pl.BlockSpec(memory_space=pl.ANY),
        scratch_shapes=[
            pltpu.VMEM((count, 4, share, width), portion.dtype),
            pltpu.SemaphoreType.DMA((4, count)),
            pltpu.SemaphoreType.DMA((4, count)),
            pltpu.SemaphoreType.DMA((2,)),
        ],
        compiler_params=pltpu.CompilerParams(
            collective_id=0, has_side_effects=True, vmem_limit_bytes=VMEM_LIMIT
        ),
        cost_estimate=pl.CostEstimate(flops=10**9, bytes_accessed=2**21, transcendentals=0),
        name="dispatch",
    )(portion)


def combine_kernel(
    count, part, weights, out, side_y, side_own, sums_y, from_y, sums, slots, pieces,
    send, recv, send_out, recv_out,
):
    row, col, partner, across, others = places_of(count)
    greet(others + [(row, partner), (row, across)])
    quarter = part.shape[2] // 4
    corner = (partner + 2) % 4

    def columns(q):
        return pl.ds(pl.multiple_of(q * quarter, quarter), quarter)

    order = list(range(1, count)) + [0]
    to_side, to_own, to_y, to_ep = {}, {}, {}, {}
    for k in order:
        target = (row + k) % count
        to_side[k] = remote(
            part.at[target, :, columns(corner)], side_y.at[k], send.at[0, k], recv.at[0, k],
            (row, partner),
        )
        to_side[k].start()
        to_own[k] = remote(
            part.at[target, :, columns(partner)], side_own.at[k], send.at[1, k], recv.at[1, k],
            (row, partner),
        )
        to_own[k].start()

    def start_y(k):
        to_y[k] = remote(
            sums_y.at[k], from_y.at[k], send.at[2, k], recv.at[2, k], (row, across)
        )
        to_y[k].start()

    def start_ep(k):
        if k:
            to_ep[k] = remote(
                sums.at[k], slots.at[row], send.at[3, k], recv.at[3, k],
                ((row + k) % count, col),
            )
            to_ep[k].start()

    for i, k in enumerate(order):
        target = (row + k) % count
        to_side[k].wait_recv()
        sums_y[k] = (
            part[target, :, columns(across)].astype(jnp.float32)
            + side_y[k].astype(jnp.float32)
        ).astype(jnp.bfloat16)
        if i:
            start_y(order[i - 1])
    to_own[order[0]].wait_recv()
    start_y(order[-1])
    for i, k in enumerate(order):
        target = (row + k) % count
        if i:
            to_own[k].wait_recv()
        mine = part[target, :, columns(col)].astype(jnp.float32) + side_own[k].astype(
            jnp.float32
        )
        to_y[k].wait_recv()
        total = (mine + from_y[k].astype(jnp.float32)).astype(jnp.bfloat16)
        if k:
            sums[k] = total
            start_ep(k)
        else:
            slots[row] = total
    table = weights[...]
    high = table.astype(jnp.bfloat16)
    low = (table - high.astype(jnp.float32)).astype(jnp.bfloat16)
    for k in order[:-1]:
        to_ep[k].wait_recv()
    rows = slots[...].reshape(-1, quarter)
    blended = jnp.dot(high, rows, preferred_element_type=jnp.float32) + jnp.dot(
        low, rows, preferred_element_type=jnp.float32
    )
    pieces[col] = blended.astype(jnp.bfloat16)
    own = pieces.at[col]
    out_y = remote(own, own, send_out.at[0], recv_out.at[0], (row, across))
    out_y.start()
    out_side = remote(own, own, send_out.at[1], recv_out.at[1], (row, partner))
    out_side.start()
    out[:, columns(col)] = pieces[col]
    out_y.wait_recv()
    other = pieces.at[across]
    out_corner = remote(other, other, send_out.at[2], recv_out.at[2], (row, partner))
    out_corner.start()
    out[:, columns(across)] = pieces[across]
    out_side.wait_recv()
    out[:, columns(partner)] = pieces[partner]
    for k in order:
        to_side[k].wait_send()
        to_own[k].wait_send()
        to_y[k].wait_send()
        if k:
            to_ep[k].wait_send()
    out_corner.wait_recv()
    out[:, columns(corner)] = pieces[corner]
    out_y.wait_send()
    out_side.wait_send()
    out_corner.wait_send()


def combine(part, weights):
    count, capacity, width = part.shape
    rows = weights.shape[0]
    quarter = width // 4
    chunk = pltpu.VMEM((count, capacity, quarter), jnp.bfloat16)
    return pl.pallas_call(
        lambda *refs: combine_kernel(count, *refs),
        out_shape=jax.ShapeDtypeStruct((rows, width), jnp.bfloat16),
        in_specs=[pl.BlockSpec(memory_space=pltpu.VMEM)] * 2,
        out_specs=pl.BlockSpec(memory_space=pltpu.VMEM),
        scratch_shapes=[chunk] * 6
        + [
            pltpu.VMEM((4, rows, quarter), jnp.bfloat16),
            pltpu.SemaphoreType.DMA((4, count)),
            pltpu.SemaphoreType.DMA((4, count)),
            pltpu.SemaphoreType.DMA((3,)),
            pltpu.SemaphoreType.DMA((3,)),
        ],
        compiler_params=pltpu.CompilerParams(
            collective_id=1, has_side_effects=True, vmem_limit_bytes=VMEM_LIMIT
        ),
        cost_estimate=pl.CostEstimate(flops=10**9, bytes_accessed=2**21, transcendentals=0),
        name="combine",
    )(part, weights)


def expert_half_kernels(
    second_batch, expert_gain, expert_choice, route_scores, expert_gate, expert_up, expert_down
):
    row_count, model_width = second_batch.shape
    experts = lax.axis_size("ep")
    capacity = 4 * row_count // experts
    share = capacity // 4
    normed = rms_scale(second_batch, expert_gain)
    names = jnp.arange(experts, dtype=jnp.int32)
    is_first = expert_choice[:, 0:1] == names[None, :]
    is_second = expert_choice[:, 1:2] == names[None, :]
    named = is_first | is_second
    rows = jnp.arange(row_count, dtype=jnp.int32)
    before = (rows[None, :] < rows[:, None]).astype(jnp.bfloat16)
    rank = jnp.dot(
        before, named.astype(jnp.bfloat16), preferred_element_type=jnp.float32
    ).astype(jnp.int32)
    rank = jnp.where(named, rank, -1)
    places = lax.axis_index("tp") * share + jnp.arange(share, dtype=jnp.int32)
    pick = (rank.T[:, None, :] == places[None, :, None]).astype(jnp.bfloat16)
    portion = (
        jnp.dot(
            pick.reshape(experts * share, row_count), normed, preferred_element_type=jnp.float32
        )
        .astype(jnp.bfloat16)
        .reshape(experts, share, model_width)
    )
    incoming = dispatch(portion).reshape(experts * capacity, model_width)
    gate_part = jnp.dot(incoming, expert_gate[0], preferred_element_type=jnp.float32)
    up_part = jnp.dot(incoming, expert_up[0], preferred_element_type=jnp.float32)
    hidden = (jax.nn.silu(gate_part) * up_part).astype(jnp.bfloat16)
    part = jnp.dot(hidden, expert_down[0], preferred_element_type=jnp.float32).astype(
        jnp.bfloat16
    )
    weight_first = jax.nn.sigmoid(route_scores[:, 0] - route_scores[:, 1])[:, None]
    weight = jnp.where(is_first, weight_first, 1.0 - weight_first)
    slot = jnp.arange(capacity, dtype=jnp.int32)
    table = jnp.where(rank[:, :, None] == slot[None, None, :], weight[:, :, None], 0.0)
    return combine(
        part.reshape(experts, capacity, model_width),
        table.reshape(row_count, experts * capacity),
    )


def per_device(
    first_batch,
    mixer_gain,
    mixer_in,
    group_maps,
    pool_scale,
    mixer_out,
    second_batch,
    expert_gain,
    expert_choice,
    route_scores,
    expert_gate,
    expert_up,
    expert_down,
):
    mixed_first = mixer_half(first_batch, mixer_gain, mixer_in, group_maps, pool_scale, mixer_out)
    small = lax.axis_size("tp") == 4 and lax.axis_size("ep") <= 8
    experts_second = (expert_half_kernels if small else expert_half)(
        second_batch, expert_gain, expert_choice, route_scores, expert_gate, expert_up, expert_down
    )
    return (mixed_first, experts_second)


def solution(mesh):
    placed = (
        P(("ep", "tp"), None),
        P(),
        P(None, "tp"),
        P(),
        P(),
        P("tp", None),
        P("ep", None),
        P(),
        P("ep", None),
        P("ep", None),
        P("ep", None, "tp"),
        P("ep", None, "tp"),
        P("ep", "tp", None),
    )
    return jax.shard_map(
        per_device,
        mesh=mesh,
        in_specs=placed,
        out_specs=(P(("ep", "tp"), None), P("ep", None)),
        check_vma=False,
    )
```

profile of v0, /device:TPU:11, one launch (start us, length us, event | category | flops | bytes accessed | tf_op | source)
XLA Modules:
  0.0 112.7 jit_solution(12098988184310742728)
XLA Ops:
  7.2 0.0 copy-start.1
  7.2 0.0 all-gather.3.cloned.1.call-start
  7.2 0.7 all-gather.3.cloned.1.call-update
  7.9 0.0 all-gather.5.cloned.1.call-start
  8.0 0.7 all-gather.5.cloned.1.call-update
  9.1 1.2 %fusion.12 = f32[128]{0:T(128)S(1)} fusion(bf16[128,2048]{1,0:T(8,128)(2,1)} %param.13), kind=kLoop, calls=%fused_computation.18 | loop fusion | flops 786304 | bytes 524800 | tf_op jit(solution)/shard_map/reduce_sum | solution.py:30
  10.3 0.8 slice_bitcast_fusion.1
  11.1 0.1 eq.232
  11.2 1.2 %fusion.15 = f32[128]{0:T(128)S(1)} fusion(bf16[128,2048]{1,0:T(8,128)(2,1)} %param.19), kind=kLoop, calls=%fused_computation.21 | loop fusion | flops 786304 | bytes 524800 | tf_op jit(solution)/shard_map/reduce_sum | solution.py:30
  12.4 0.1 bitcast_select_fusion
  12.6 0.0 copy-done.5
  12.6 0.1 bitcast_compare_fusion
  12.8 0.4 convolution_convert_fusion
  13.1 30.7 %dispatch.1 = bf16[8,4,16,2048]{3,2,1,0:T(8,128)(2,1)S(1)} custom-call(bf16[8,16,2048]{2,1,0:T(8,128)(2,1)S(1)} %bitcast.41), custom_call_target="tpu_custom_call" | custom-call | flops 1000000000 | bytes 2097152 | tf_op jit(solution)/shard_map/dispatch/pallas_call | solution.py:212
  43.8 0.0 copy-start.3
  43.9 0.1 copy.17
  44.0 0.1 copy.18
  44.2 0.1 eq.238
  44.3 0.4 copy-done.3
  44.7 1.2 %multiply_bitcast_fusion = bf16[8,64,8,64]{3,2,1,0:T(8,128)(2,1)} fusion(bf16[8,64,64]{2,1,0:T(8,128)(2,1)S(1)} %copy-done.3, bf16[8,8]{1,0:T(8,128)(2,1)S(1)} %fusion.145), kind=kLoop, calls=%fused_computation.24 | loop fusion | flops 262144 | bytes 589952 | tf_op jit(solution)/shard_map/gcd,gh->gchd/transpose | solution.py:66
  46.0 5.7 %fusion.4 = f32[512,896]{1,0:T(8,128)} fusion(bf16[512,2048]{1,0:T(8,128)(2,1)S(1)} %bitcast.42, bf16[1,2048,896]{2,1,0:T(8,128)(2,1)} %param.23), kind=kOutput, calls=%fused_computation.4 | convolution fusion | flops 1879048192 | bytes 7602176 | tf_op jit(solution)/shard_map/dot_general | solution.py:387
  51.6 9.7 %fusion.6 = bf16[512,2048]{1,0:T(8,128)(2,1)} fusion(bf16[1,896,2048]{2,1,0:T(8,128)(2,1)} %param.25, f32[512,896]{1,0:T(8,128)} %fusion.4, bf16[512,2048]{1,0:T(8,128)(2,1)S(1)} %bitcast.43, bf16[1,2048,896]{2,1,0:T(8,128)(2,1)} %param.24), kind=kOutput, calls=%fused_computation.6 | convolution fusion | flops 3761897472 | bytes 13369344 | tf_op jit(solution)/shard_map/dot_general | solution.py:390
  61.3 2.2 %convolution_convert_fusion.2 = bf16[128,512]{1,0:T(8,128)(2,1)S(1)} fusion(bf16[2048,512]{1,0:T(8,128)(2,1)} %all-gather.3.cloned.1.call-done, bf16[128,2048]{1,0:T(8,128)(2,1)S(1)} %copy-done.2, f32[2048]{0:T(1024)S(1)} %copy-done.6, f32[128]{0:T(128)S(1)} %add_rsqrt_fusion.1), kind=kOutput, calls=%fused_computation.16 | convolution fusion | flops 269549568 | bytes 2761216 | tf_op jit(solution)/shard_map/dot_general | solution.py:37
  63.5 2.4 %collective-permute-start = (bf16[8,512]{1,0:T(8,128)(2,1)S(1)}, bf16[8,512]{1,0:T(8,128)(2,1)S(1)}, u32[]{:S(2)}, u32[]{:S(2)}) collective-permute-start(bf16[8,512]{1,0:T(8,128)(2,1)S(1)} %get-tuple-element.4), channel_id=1, source_target_pairs={{0,1},{1,2},{2,3},{3,4},{4,5},{5,6},{6,7},{7,8},{8,9},{9,10},{10,1... | collective-permute-start | bytes 24584 | tf_op jit(solution)/shard_map/ppermute | solution.py:20
  65.9 2.0 %collective-permute-start.1 = (bf16[8,512]{1,0:T(8,128)(2,1)S(1)}, bf16[8,512]{1,0:T(8,128)(2,1)S(1)}, u32[]{:S(2)}, u32[]{:S(2)}) collective-permute-start(bf16[8,512]{1,0:T(8,128)(2,1)S(1)} %get-tuple-element.5), channel_id=1, source_target_pairs={{1,0},{2,1},{3,2},{4,3},{5,4},{6,5},{7,6},{8,7},{9,8},{10,9},{11,1... | collective-permute-start | bytes 24584 | tf_op jit(solution)/shard_map/ppermute | solution.py:23
  67.9 0.0 copy-start.7
  67.9 30.9 %combine.1 = bf16[128,2048]{1,0:T(8,128)(2,1)S(1)} custom-call(bf16[8,64,2048]{2,1,0:T(8,128)(2,1)S(1)} %bitcast.44, f32[128,512]{1,0:T(8,128)S(1)} %compare_select_fusion.refs_1_), custom_call_target="tpu_custom_call" | custom-call | flops 1000000000 | bytes 2097152 | tf_op jit(solution)/shard_map/combine/pallas_call | solution.py:338
  98.8 1.9 %reshape.526 = bf16[512,512]{1,0:T(8,128)(2,1)S(1)} reshape(bf16[8,64,8,64]{3,2,1,0:T(8,128)(2,1)} %multiply_bitcast_fusion) | data formatting | bytes 1048576 | tf_op jit(solution)/shard_map/reshape | solution.py:66
  100.7 0.0 collective-permute-done
  100.8 0.0 all-gather.5.cloned.1.call-done
  100.8 4.3 %convolution_convert_fusion.1 = bf16[128,2048]{1,0:T(8,128)(2,1)} fusion(bf16[512,2048]{1,0:T(8,128)(2,1)} %all-gather.5.cloned.1.call-done, bf16[512,512]{1,0:T(8,128)(2,1)S(1)} %reshape.526, f32[144,512]{1,0:T(8,128)S(1)} %maximum_convert_fusion, f32[512]{0:T(512)S(1)} %copy-done.7, f32[512]{0:T(512)S(1)} %get-tuple-element.55, ...), kind=kOutput, calls=%fused_computation.8 | convolution fusion | flops 342097920 | bytes 7367680 | tf_op jit(solution)/shard_map/dot_general | solution.py:70
  105.1 0.8 copy.22
  (51 shorter events, 0.4 us)
Async XLA Ops:
  7.2 5.6 %copy-start.1 = (bf16[128,2048]{1,0:T(8,128)(2,1)S(1)}, bf16[128,2048]{1,0:T(8,128)(2,1)}, u32[]{:S(2)}) copy-start(bf16[128,2048]{1,0:T(8,128)(2,1)} %param.19) | copy-start | bytes 1572868
  7.2 5.4 %copy-start.5 = (f32[128,2]{0,1:T(2,128)S(1)}, f32[128,2]{0,1:T(2,128)}, u32[]{:S(2)}) copy-start(f32[128,2]{0,1:T(2,128)} %param.22) | copy-start | bytes 3076
  7.2 5.6 %copy-start.4 = (f32[2048]{0:T(1024)S(1)}, f32[2048]{0:T(1024)}, u32[]{:S(2)}) copy-start(f32[2048]{0:T(1024)} %param.20) | copy-start | bytes 24580
  7.2 54.1 %all-gather.3.cloned.1.call-start = ((), (), s32[]{:S(2)}) async-start(), calls=%async_computation | async-start | bytes 2621440 | tf_op jit(solution)/shard_map/all_gather | solution.py:39
  7.9 92.9 %all-gather.5.cloned.1.call-start = ((), (), s32[]{:S(2)}) async-start(), calls=%async_computation.1 | async-start | bytes 2621440 | tf_op jit(solution)/shard_map/all_gather | solution.py:72
  43.8 0.9 copy-start.3
  51.6 9.7 %copy-start.2 = (bf16[128,2048]{1,0:T(8,128)(2,1)S(1)}, bf16[128,2048]{1,0:T(8,128)(2,1)}, u32[]{:S(2)}) copy-start(bf16[128,2048]{1,0:T(8,128)(2,1)} %param.13) | copy-start | bytes 1572868
  51.6 9.7 %copy-start.6 = (f32[2048]{0:T(1024)S(1)}, f32[2048]{0:T(1024)}, u32[]{:S(2)}) copy-start(f32[2048]{0:T(1024)} %param.14) | copy-start | bytes 24580
  61.3 6.6 %copy-start = (bf16[512,2048]{1,0:T(8,128)(2,1)S(1)}, bf16[512,2048]{1,0:T(8,128)(2,1)}, u32[]{:S(2)}) copy-start(bf16[512,2048]{1,0:T(8,128)(2,1)} %fusion.6) | copy-start | bytes 6291460
  63.5 37.2 %collective-permute-start = (bf16[8,512]{1,0:T(8,128)(2,1)S(1)}, bf16[8,512]{1,0:T(8,128)(2,1)S(1)}, u32[]{:S(2)}, u32[]{:S(2)}) collective-permute-start(bf16[8,512]{1,0:T(8,128)(2,1)S(1)} %get-tuple-element.4), channel_id=1, source_target_pairs={{0,1},{1,2},{2,3},{3,4},{4,5},{5,6},{6,7},{7,8},{8,9},{9,10},{10,1... | collective-permute-start | bytes 24584 | tf_op jit(solution)/shard_map/ppermute | solution.py:20
  65.9 34.8 %collective-permute-start.1 = (bf16[8,512]{1,0:T(8,128)(2,1)S(1)}, bf16[8,512]{1,0:T(8,128)(2,1)S(1)}, u32[]{:S(2)}, u32[]{:S(2)}) collective-permute-start(bf16[8,512]{1,0:T(8,128)(2,1)S(1)} %get-tuple-element.5), channel_id=1, source_target_pairs={{1,0},{2,1},{3,2},{4,3},{5,4},{6,5},{7,6},{8,7},{9,8},{10,9},{11,1... | collective-permute-start | bytes 24584 | tf_op jit(solution)/shard_map/ppermute | solution.py:23
  67.9 32.9 %copy-start.7 = (f32[512]{0:T(512)S(1)}, f32[512]{0:T(512)}, u32[]{:S(2)}) copy-start(f32[512]{0:T(512)} %param.17) | copy-start | bytes 6148
Sparse Core Ops, SparseCore 0:
  9.6 34.0 all-gather.2
  45.3 20.7 all-gather.4
where the time goes:
time: 113 us
  Pallas kernels  61.6 us (55%)
  matrix products  22.3 us (20%)
  between operations  14.5 us (13%)
  local copies, waits for them, and re-layouts  4.4 us (4%)
  starting transfers between devices  4.4 us (4%)
  other arithmetic  4.15 us (4%)
  waiting for transfers between devices  1.4 us (1%)
    pallas_call x1, Pallas kernels, combine(): pl.pallas_call(lambda *refs: combine_kernel(count, *refs), out_shape=jax....  30.9 us
    pallas_call x1, Pallas kernels, dispatch(): pl.pallas_call(lambda *refs: dispatch_kernel(count, *refs), out_shape=jax...  30.7 us
    dot_general x1, matrix products, expert_half_kernels(): jnp.dot(hidden, expert_down[0], preferred_element_type=jnp.float32)  9.65 us
    dot_general x1, matrix products, expert_half_kernels(): jnp.dot(incoming, expert_gate[0], preferred_element_type=jnp.float32)  5.65 us
    dot_general x1, matrix products, mixer_half(): jnp.dot(grouped, lax.all_gather(mixer_out, 'tp', axis=0, tiled=True), pre...  4.26 us
    reduce_sum x2, other arithmetic, rms_scale(): jnp.mean(floats * floats, axis=-1, keepdims=True) + epsilon  2.46 us
    ppermute x1, starting transfers between devices, extended(): lax.ppermute(lax.slice_in_dim(block, block.shape[dim] - width, None, axis...  2.35 us
  transfers between devices with their start and end apart: 4, of which 0 were waited for; matrix products, arithmetic and copies ran while one was open for 22% of the time, Pallas kernels for 55%

commit v1 on v0

v1 whole, which is shorter than its diff:
```python
import jax
import jax.numpy as jnp
from jax import lax
from jax.experimental import pallas as pl
from jax.experimental.pallas import tpu as pltpu
from jax.sharding import PartitionSpec as P

GROUP = 64
SEQS = 1


epsilon = 1e-06


def extended(block, sides, width):
    for axis, dim in sides:
        count = lax.axis_size(axis)
        forward = [(i, i + 1) for i in range(count - 1)]
        backward = [(target, source) for source, target in forward]
        low = lax.ppermute(
            lax.slice_in_dim(block, block.shape[dim] - width, None, axis=dim), axis, forward
        )
        high = lax.ppermute(lax.slice_in_dim(block, 0, width, axis=dim), axis, backward)
        block = jnp.concatenate([low, block, high], axis=dim)
    return block


def rms_scale(values, gain):
    floats = values.astype(jnp.float32)
    factor = lax.rsqrt(jnp.mean(floats * floats, axis=-1, keepdims=True) + epsilon)
    return (floats * factor * gain).astype(jnp.bfloat16)


def mixer_half(first_batch, mixer_gain, mixer_in, group_maps, pool_scale, mixer_out):
    count_rows = first_batch.shape[0]
    normed = rms_scale(first_batch, mixer_gain)
    pooled_in = jnp.dot(
        normed,
        lax.all_gather(mixer_in, "tp", axis=1, tiled=True),
        preferred_element_type=jnp.float32,
    ).astype(jnp.bfloat16)
    channels = pooled_in.shape[1]
    padded = extended(pooled_in, ((("ep", "tp"), 0),), 8).astype(jnp.float32)
    devices = lax.axis_size("ep") * lax.axis_size("tp")
    seq_length = count_rows * devices // SEQS
    first_row = (lax.axis_index("ep") * lax.axis_size("tp") + lax.axis_index("tp")) * count_rows
    places = first_row + jnp.arange(count_rows, dtype=jnp.int32)
    own_seq = places // seq_length
    group_of = jnp.arange(channels, dtype=jnp.int32) // GROUP
    half_span = jnp.left_shift(jnp.ones_like(group_of), group_of % 4)
    window_sum = jnp.zeros((count_rows, channels), jnp.float32)
    window_count = jnp.zeros((count_rows, channels), jnp.float32)
    for offset in range(-8, 8):
        inside = (
            ((places + offset) // seq_length == own_seq)[:, None]
            & (offset >= -half_span)[None, :]
            & (offset < half_span)[None, :]
        )
        window_sum = window_sum + jnp.where(
            inside, padded[8 + offset : 8 + offset + count_rows], 0.0
        )
        window_count = window_count + inside.astype(jnp.float32)
    centred = (window_sum / window_count - padded[8 : 8 + count_rows]).astype(jnp.bfloat16)
    group_count = group_maps.shape[0]
    identity = jnp.eye(group_count, dtype=jnp.bfloat16)
    block_map = jnp.einsum("gcd,gh->gchd", group_maps, identity).reshape(channels, channels)
    grouped = (jnp.dot(centred, block_map, preferred_element_type=jnp.float32) * pool_scale).astype(
        jnp.bfloat16
    )
    mixed_out = jnp.dot(
        grouped,
        lax.all_gather(mixer_out, "tp", axis=0, tiled=True),
        preferred_element_type=jnp.float32,
    )
    return mixed_out.astype(jnp.bfloat16)


def expert_half(
    second_batch, expert_gain, expert_choice, route_scores, expert_gate, expert_up, expert_down
):
    row_count = second_batch.shape[0]
    model_width = second_batch.shape[1]
    experts = lax.axis_size("ep")
    tp_count = lax.axis_size("tp")
    capacity = 4 * row_count // experts
    share = capacity // tp_count
    normed = rms_scale(second_batch, expert_gain)
    chosen = expert_choice.reshape(-1)
    one_hot = (chosen[:, None] == jnp.arange(experts, dtype=jnp.int32)[None, :]).astype(jnp.int32)
    ranking = jnp.sum(jnp.cumsum(one_hot, axis=0) * one_hot, axis=1) - 1
    slot_place = ranking * experts + chosen
    source_row = jnp.arange(chosen.shape[0], dtype=jnp.int32) // expert_choice.shape[1]
    slot_table = jnp.zeros((capacity * experts,), jnp.int32).at[slot_place].set(source_row + 1)
    outgoing = jnp.where(
        (slot_table > 0)[:, None],
        normed[jnp.maximum(slot_table - 1, 0)],
        jnp.zeros((), jnp.bfloat16),
    )
    outgoing = outgoing.reshape(capacity, experts, model_width)
    portion = lax.dynamic_slice_in_dim(outgoing, lax.axis_index("tp") * share, share, 0)
    arrived_part = lax.all_to_all(portion, "ep", split_axis=1, concat_axis=1, tiled=True)
    arrived = lax.all_gather(arrived_part, "tp", axis=0, tiled=True)
    incoming = arrived.reshape(capacity * experts, model_width)
    gate_weight = expert_gate[0]
    up_weight = expert_up[0]
    down_weight = expert_down[0]
    gate_part = jnp.dot(incoming, gate_weight, preferred_element_type=jnp.float32)
    up_part = jnp.dot(incoming, up_weight, preferred_element_type=jnp.float32)
    hidden = (jax.nn.silu(gate_part) * up_part).astype(jnp.bfloat16)
    summed = lax.psum_scatter(
        jnp.dot(hidden, down_weight, preferred_element_type=jnp.float32).astype(jnp.bfloat16),
        "tp",
        scatter_dimension=0,
        tiled=True,
    )
    finished = summed.reshape(share, experts, model_width)
    returned = lax.all_to_all(finished, "ep", split_axis=1, concat_axis=1, tiled=True)
    every_slot = lax.all_gather(returned, "tp", axis=0, tiled=True).reshape(
        capacity * experts, model_width
    )
    picked = every_slot[slot_place].reshape(row_count, -1, model_width)
    weight_first = jax.nn.sigmoid(route_scores[:, 0] - route_scores[:, 1])[:, None]
    blended = weight_first * picked[:, 0].astype(jnp.float32) + (1.0 - weight_first) * picked[
        :, 1
    ].astype(jnp.float32)
    return blended.astype(jnp.bfloat16)


MESH = pl.DeviceIdType.MESH
VMEM_LIMIT = 60 * 1024 * 1024
F32 = jnp.float32
BF16 = jnp.bfloat16


def flip(row, relation):
    place = row
    for bit in (1, 2, 4):
        if relation & bit:
            place = place + bit * (1 - 2 * ((row // bit) % 2))
    return place


def weave(main, extra):
    taken = 0
    for i, step in enumerate(main):
        step()
        due = (i + 1) * len(extra) // len(main)
        while taken < due:
            extra[taken]()
            taken += 1


def normalize(source, gain, target):
    for i in range(0, source.shape[0], 16):
        floats = source[i : i + 16].astype(F32)
        factor = lax.rsqrt(jnp.mean(floats * floats, axis=-1, keepdims=True) + epsilon)
        target[i : i + 16] = (floats * factor * gain[...]).astype(BF16)


def layer_kernel(
    first_hbm, mixer_gain_hbm, mixer_in_hbm, maps_hbm, scale_hbm, mixer_out_hbm,
    second_hbm, expert_gain_hbm, choice_hbm, scores_hbm, gate_hbm, up_hbm, down_hbm,
    mixed_hbm, result_hbm,
    x1, x2, n1, n2, gain1, gain2, scale, choice, scores, maps,
    w_in, w_down, m1, m2,
    rank_of, pick, portion, landed, hidden, part,
    side_y, side_own, sums_y, from_y, sums, slots, high, low, pieces,
    padded, floats, grouped, mixed,
    load, d_send, d_recv, c_send, c_recv, m_send, m_recv, h_send, h_recv, f_send, f_recv, store,
):
    row, col = lax.axis_index("ep"), lax.axis_index("tp")
    count = landed.shape[0]
    share = landed.shape[2]
    capacity = 4 * share
    rows, width = x2.shape
    quarter = width // 4
    tiles = w_in.shape[0]
    shard = m1.shape[1] // 4
    partner = col + 1 - 2 * (col % 2)
    across = (col + 2) % 4
    corner = (partner + 2) % 4
    devices = 4 * count
    index = row * 4 + col
    after, before = (index + 1) % devices, (index + devices - 1) % devices
    after_device, before_device = (after // 4, after % 4), (before // 4, before % 4)
    peer = [(flip(row, k), col) for k in range(count)]
    on_chip, over_y = (row, partner), (row, across)

    def remote(source, target, send, recv, device):
        return pltpu.make_async_remote_copy(
            src_ref=source, dst_ref=target, send_sem=send, recv_sem=recv,
            device_id=device, device_id_type=MESH,
        )

    def shard_of(which):
        return pl.ds(pl.multiple_of(which * shard, shard), shard)

    loads = {}

    def fetch(name, source, target):
        loads[name] = pltpu.make_async_copy(source, target, load.at[len(loads)])
        loads[name].start()

    fetch("x2", second_hbm, x2)
    fetch("gain2", expert_gain_hbm, gain2)
    fetch("choice", choice_hbm, choice)
    fetch("scores", scores_hbm, scores)
    fetch("m1", mixer_in_hbm, m1.at[:, shard_of(col)])
    fetch("m2", mixer_out_hbm, m2.at[shard_of(col)])
    fetch("x1", first_hbm, x1)
    fetch("gain1", mixer_gain_hbm, gain1)
    fetch("maps", maps_hbm, maps)
    fetch("scale", scale_hbm, scale)
    for j in range(tiles):
        fetch(f"gate{j}", gate_hbm.at[0, :, pl.ds(128 * j, 128)], w_in.at[j, :, pl.ds(0, 128)])
        fetch(f"up{j}", up_hbm.at[0, :, pl.ds(128 * j, 128)], w_in.at[j, :, pl.ds(128, 128)])
    fetch("down", down_hbm.at[0], w_down)

    barrier = pltpu.get_barrier_semaphore()
    peers = peer[1:] + [on_chip, over_y, after_device, before_device]
    for device in peers:
        pl.semaphore_signal(barrier, inc=1, device_id=device, device_id_type=MESH)

    loads["choice"].wait()
    experts = lax.broadcasted_iota(jnp.int32, (16, rows), 0)
    first, second = choice[0:1], choice[1:2]
    named = (first == experts) | (second == experts)
    earlier = lax.broadcasted_iota(jnp.int32, (rows, rows), 0) < lax.broadcasted_iota(
        jnp.int32, (rows, rows), 1
    )
    rank = jnp.dot(
        named.astype(F32).astype(BF16), earlier.astype(F32).astype(BF16), preferred_element_type=F32
    )
    rank_of[...] = jnp.where(named, rank, -1.0)

    def rank_at(k):
        return rank_of[pl.ds(peer[k][0], 1), :]

    place = lax.broadcasted_iota(jnp.int32, (capacity, rows), 0).astype(F32)
    offset = (col * share).astype(F32)
    for k in range(1, count):
        chosen = place[:share] + offset == rank_at(k)
        pick[(k - 1) * share : k * share] = chosen.astype(F32).astype(BF16)
    own = (count - 1) * share
    pick[own:] = (place == rank_at(0)).astype(F32).astype(BF16)

    loads["x2"].wait()
    loads["gain2"].wait()
    normalize(x2, gain2, n2)
    for n in range(0, width, 256):
        taken = jnp.dot(pick[...], n2[:, n : n + 256], preferred_element_type=F32).astype(BF16)
        portion[:, :, n : n + 256] = taken[:own].reshape(count - 1, share, 256)
        landed[0, :, :, n : n + 256] = taken[own:].reshape(4, share, 256)

    loads["m1"].wait()
    loads["m2"].wait()
    pl.semaphore_wait(barrier, len(peers))

    firsts, ys, sides, corners = {}, {}, {}, {}
    for k in FIRST_ORDER:
        firsts[k] = remote(
            portion.at[k - 1], landed.at[k, col], d_send.at[0, k], d_recv.at[0, k], peer[k]
        )
        firsts[k].start()

    def forward(k):
        def run():
            firsts[k].wait_recv()
            block = landed.at[k, col]
            ys[k] = remote(block, block, d_send.at[1, k], d_recv.at[1, k], over_y)
            ys[k].start()
            sides[k] = remote(block, block, d_send.at[2, k], d_recv.at[2, k], on_chip)
            sides[k].start()

        return run

    def turn(k):
        def run():
            ys[k].wait_recv()
            block = landed.at[k, across]
            corners[k] = remote(block, block, d_send.at[3, k], d_recv.at[3, k], on_chip)
            corners[k].start()

        return run

    fourth = row % 4
    moves = []

    def piece(which, owner, start, size):
        if which == 0:
            unit = m1.shape[0] // 4
            return m1.at[pl.ds(pl.multiple_of(start * unit, unit), size * unit), shard_of(owner)]
        unit = shard // 4
        return m2.at[pl.ds(pl.multiple_of(owner * shard + start * unit, unit), size * unit)]

    def move(which, kind, owner, start, size, device):
        block = piece(which, owner, start, size)
        copy = remote(block, block, m_send.at[which, kind], m_recv.at[which, kind], device)
        copy.start()
        moves.append(copy)
        return copy

    own_shard, by_y, by_x, by_z, pass_y, pass_x, pass_z = {}, {}, {}, {}, {}, {}, {}
    for w in range(2):
        by_y[w] = move(w, 0, col, fourth, 1, over_y)
    for w in range(2):
        own_shard[w] = move(w, 1, col, 0, 4, on_chip)

    def spread_x(w):
        def run():
            by_y[w].wait_recv()
            by_x[w] = move(w, 2, across, fourth, 1, peer[1])
            pass_y[w] = move(w, 3, across, fourth, 1, on_chip)

        return run

    def spread_z(w):
        def run():
            by_x[w].wait_recv()
            other = fourth + 1 - 2 * (fourth % 2)
            by_z[w] = move(w, 4, across, 2 * (fourth // 2), 2, peer[2])
            pass_x[w] = move(w, 5, across, other, 1, on_chip)

        return run

    def pass_on(w):
        def run():
            by_z[w].wait_recv()
            pass_z[w] = move(w, 6, across, 2 - 2 * (fourth // 2), 2, on_chip)

        return run

    def gathered(w):
        for copy in (own_shard[w], pass_y[w], pass_x[w], pass_z[w]):
            copy.wait_recv()

    def make_table():
        loads["scores"].wait()
        weight_first = jax.nn.sigmoid(scores[0:1] - scores[1:2])
        for k in range(0, count, 2):
            blocks = []
            for i in (k, k + 1):
                weight = jnp.where(first == peer[i][0], weight_first, 1.0 - weight_first)
                blocks.append(jnp.where(place == rank_at(i), weight, 0.0))
            table = jnp.concatenate(blocks, axis=0).T
            top = table.astype(BF16)
            columns = slice(k * capacity, (k + 2) * capacity)
            high[:, columns] = top
            low[:, columns] = (table - top.astype(F32)).astype(BF16)

    def arrive(start, stop):
        def run():
            for k in range(max(start, 1), stop):
                sides[k].wait_recv()
                corners[k].wait_recv()

        return run

    weights_ready = set()

    def ready(name):
        if name not in weights_ready:
            weights_ready.add(name)
            loads[name].wait()

    to_side, to_own, to_y, to_ep = {}, {}, {}, {}

    def expert_steps(start, stop):
        size = (stop - start) * capacity

        def up(j):
            def run():
                ready(f"gate{j}")
                ready(f"up{j}")
                both = jnp.dot(
                    landed[start:stop].reshape(size, width), w_in[j], preferred_element_type=F32
                )
                gate = both[:, :128]
                hidden[:size, 128 * j : 128 * j + 128] = (
                    gate / (1.0 + jnp.exp(-gate)) * both[:, 128:]
                ).astype(BF16)

            return run

        def down(i, which):
            def run():
                ready("down")
                for h in range(0, quarter, 256):
                    columns = pl.ds(pl.multiple_of(which * quarter + h, 256), 256)
                    part[start:stop, i, :, h : h + 256] = (
                        jnp.dot(hidden[:size], w_down[:, columns], preferred_element_type=F32)
                        .astype(BF16)
                        .reshape(stop - start, capacity, 256)
                    )
                for k in range(start, stop):
                    if i == 1:
                        to_side[k] = remote(
                            part.at[k, 0], side_y.at[k], c_send.at[0, k], c_recv.at[0, k], on_chip
                        )
                        to_side[k].start()
                    if i == 2:
                        to_own[k] = remote(
                            part.at[k, 1], side_own.at[k], c_send.at[1, k], c_recv.at[1, k], on_chip
                        )
                        to_own[k].start()

            return run

        return [up(j) for j in range(tiles)] + [
            down(i, q) for i, q in enumerate((corner, partner, across, col))
        ]

    def add_y(ks):
        def run():
            for k in ks:
                to_side[k].wait_recv()
                sums_y[k] = (part[k, 2].astype(F32) + side_y[k].astype(F32)).astype(BF16)
            for k in ks:
                to_y[k] = remote(
                    sums_y.at[k], from_y.at[k], c_send.at[2, k], c_recv.at[2, k], over_y
                )
                to_y[k].start()

        return run

    def add_all(ks):
        def run():
            for k in ks:
                to_own[k].wait_recv()
                to_y[k].wait_recv()
                total = (
                    part[k, 3].astype(F32) + side_own[k].astype(F32) + from_y[k].astype(F32)
                ).astype(BF16)
                if k:
                    sums[k] = total
                else:
                    slots[0] = total
            for k in ks:
                if k:
                    to_ep[k] = remote(
                        sums.at[k], slots.at[k], c_send.at[3, k], c_recv.at[3, k], peer[k]
                    )
                    to_ep[k].start()

        return run

    halo = {}

    def mix_norm():
        loads["x1"].wait()
        loads["gain1"].wait()
        normalize(x1, gain1, n1)

    def mix_in():
        gathered(0)
        for n in range(0, m1.shape[1], 256):
            padded[16 : 16 + rows, n : n + 256] = jnp.dot(
                n1[...], m1[:, n : n + 256], preferred_element_type=F32
            ).astype(BF16)

    def mix_edges():
        halo[0] = remote(
            padded.at[pl.ds(rows, 16)], padded.at[pl.ds(0, 16)], h_send.at[0], h_recv.at[0],
            after_device,
        )
        halo[0].start()
        halo[1] = remote(
            padded.at[pl.ds(16, 16)], padded.at[pl.ds(16 + rows, 16)], h_send.at[1], h_recv.at[1],
            before_device,
        )
        halo[1].start()

    def mix_centre():
        halo[0].wait_recv()
        halo[1].wait_recv()
        loads["maps"].wait()
        loads["scale"].wait()
        seq_length = rows * devices // SEQS
        opening = (index * rows) % seq_length
        keep_low = (opening > 0).astype(F32)
        keep_high = (opening + rows < seq_length).astype(F32)
        floats[16 : 16 + rows] = padded[16 : 16 + rows].astype(F32)
        low_rows, high_rows = padded[:16].astype(F32), padded[16 + rows :].astype(F32)
        floats[:16] = jnp.where(keep_low > 0, low_rows, 0.0)
        floats[16 + rows :] = jnp.where(keep_high > 0, high_rows, 0.0)
        position = opening + lax.broadcasted_iota(jnp.int32, (rows, 128), 0)
        lane = lax.broadcasted_iota(jnp.int32, (rows, 128), 1)
        line = lax.broadcasted_iota(jnp.int32, (128, 128), 0)
        across_lane = lax.broadcasted_iota(jnp.int32, (128, 128), 1)
        copies = (
            lax.broadcasted_iota(jnp.int32, (GROUP, 128), 0)
            == lax.broadcasted_iota(jnp.int32, (GROUP, 128), 1) % GROUP
        ).astype(F32).astype(BF16)
        for b in range(padded.shape[1] // 128):
            columns = slice(128 * b, 128 * b + 128)

            def window(span):
                total = floats[16 - span : 16 - span + rows, columns]
                for step in range(-span + 1, span):
                    total = total + floats[16 + step : 16 + step + rows, columns]
                held = jnp.minimum(position + span, seq_length) - jnp.maximum(position - span, 0)
                return total / held.astype(F32)

            small = 1 if b % 2 == 0 else 4
            mean = jnp.where(lane < GROUP, window(small), window(2 * small))
            centred = (mean - floats[16 : 16 + rows, columns]).astype(BF16)
            spread = jnp.dot(maps[columns], copies, preferred_element_type=F32)
            block = jnp.where(line // GROUP == across_lane // GROUP, spread, 0.0).astype(BF16)
            grouped[:, columns] = (
                jnp.dot(centred, block, preferred_element_type=F32) * scale[:, columns]
            ).astype(BF16)

    def mix_out():
        gathered(1)
        for n in range(0, width, 256):
            mixed[:, n : n + 256] = jnp.dot(
                grouped[...], m2[:, n : n + 256], preferred_element_type=F32
            ).astype(BF16)

    stores = []

    def keep(source, target):
        copy = pltpu.make_async_copy(source, target, store.at[len(stores)])
        copy.start()
        stores.append(copy)

    run_schedule(
        forward, turn, spread_x, spread_z, pass_on, make_table, arrive, expert_steps, add_y,
        add_all, mix_norm, mix_in, mix_edges, mix_centre, mix_out,
        lambda: keep(mixed, mixed_hbm),
    )

    for k in EP_ORDER:
        to_ep[k].wait_recv()
    half = rows // 2
    out_y, out_side, out_corner = {}, {}, {}
    for h in range(2):
        held = slice(h * half, h * half + half)
        returned = slots[...].reshape(count * capacity, quarter)
        pieces[col, held] = (
            jnp.dot(high[held], returned, preferred_element_type=F32)
            + jnp.dot(low[held], returned, preferred_element_type=F32)
        ).astype(BF16)
    for h in range(2):
        block = pieces.at[col, pl.ds(h * half, half)]
        out_y[h] = remote(block, block, f_send.at[0, h], f_recv.at[0, h], over_y)
        out_y[h].start()
    for h in range(2):
        block = pieces.at[col, pl.ds(h * half, half)]
        out_side[h] = remote(block, block, f_send.at[1, h], f_recv.at[1, h], on_chip)
        out_side[h].start()

    def quarter_of(which):
        return result_hbm.at[:, pl.ds(pl.multiple_of(which * quarter, quarter), quarter)]

    keep(pieces.at[col], quarter_of(col))
    for h in range(2):
        out_y[h].wait_recv()
        block = pieces.at[across, pl.ds(h * half, half)]
        out_corner[h] = remote(block, block, f_send.at[2, h], f_recv.at[2, h], on_chip)
        out_corner[h].start()
    keep(pieces.at[across], quarter_of(across))
    for h in range(2):
        out_side[h].wait_recv()
    keep(pieces.at[partner], quarter_of(partner))
    for h in range(2):
        out_corner[h].wait_recv()
    keep(pieces.at[corner], quarter_of(corner))

    for k in range(count):
        to_side[k].wait_send()
        to_own[k].wait_send()
        to_y[k].wait_send()
        if k:
            firsts[k].wait_send()
            ys[k].wait_send()
            sides[k].wait_send()
            corners[k].wait_send()
            to_ep[k].wait_send()
    for copy in moves:
        copy.wait_send()
    for i in range(2):
        halo[i].wait_send()
        out_y[i].wait_send()
        out_side[i].wait_send()
        out_corner[i].wait_send()
    for copy in stores:
        copy.wait()


FIRST_ORDER = (4, 5, 1, 2, 3, 6, 7)
EP_ORDER = (1, 2, 3, 4, 5, 6, 7)


def run_schedule(
    forward, turn, spread_x, spread_z, pass_on, make_table, arrive, expert_steps, add_y,
    add_all, mix_norm, mix_in, mix_edges, mix_centre, mix_out, keep_mixed,
):
    make_table()
    mix_norm()
    for step in (forward(1), forward(4), forward(2), turn(1), forward(3), spread_x(0)):
        step()
    arrive(0, 2)()
    weave(expert_steps(0, 2), [turn(2), forward(5), turn(3), spread_x(1)])
    arrive(2, 4)()
    weave(expert_steps(2, 4), [turn(4), add_y((1, 0)), forward(6), turn(5)])
    arrive(4, 6)()
    weave(
        expert_steps(4, 6),
        [add_y((2, 3)), forward(7), turn(6), add_all((1, 0)), spread_z(0), spread_z(1), turn(7)],
    )
    arrive(6, 8)()
    weave(expert_steps(6, 8), [add_y((4, 5)), add_all((2, 3))])
    add_all((4, 5))()
    add_y((6, 7))()
    pass_on(0)()
    add_all((6, 7))()
    mix_in()
    mix_edges()
    pass_on(1)()
    mix_centre()
    mix_out()
    keep_mixed()


def fused(
    first_batch, mixer_gain, mixer_in, group_maps, pool_scale, mixer_out,
    second_batch, expert_gain, expert_choice, route_scores, expert_gate, expert_up, expert_down,
):
    rows, width = second_batch.shape
    count = lax.axis_size("ep")
    channels = pool_scale.shape[0]
    ff = expert_gate.shape[2]
    share = rows // count
    capacity = 4 * share
    quarter = width // 4
    tiles = ff // 128
    chunk = pltpu.VMEM((count, capacity, quarter), BF16)
    dma = pltpu.SemaphoreType.DMA
    anywhere = pl.BlockSpec(memory_space=pl.ANY)
    operands = (
        first_batch, mixer_gain.reshape(1, width), mixer_in,
        group_maps.reshape(channels, GROUP), pool_scale.reshape(1, channels), mixer_out,
        second_batch, expert_gain.reshape(1, width), expert_choice.T, route_scores.T,
        expert_gate, expert_up, expert_down,
    )
    return pl.pallas_call(
        layer_kernel,
        out_shape=(
            jax.ShapeDtypeStruct(first_batch.shape, BF16),
            jax.ShapeDtypeStruct(second_batch.shape, BF16),
        ),
        in_specs=[anywhere] * len(operands),
        out_specs=(anywhere, anywhere),
        scratch_shapes=[
            pltpu.VMEM((rows, width), BF16),
            pltpu.VMEM((rows, width), BF16),
            pltpu.VMEM((rows, width), BF16),
            pltpu.VMEM((rows, width), BF16),
            pltpu.VMEM((1, width), F32),
            pltpu.VMEM((1, width), F32),
            pltpu.VMEM((1, channels), F32),
            pltpu.VMEM((2, rows), jnp.int32),
            pltpu.VMEM((2, rows), F32),
            pltpu.VMEM((channels, GROUP), BF16),
            pltpu.VMEM((tiles, width, 256), BF16),
            pltpu.VMEM((ff, width), BF16),
            pltpu.VMEM((width, channels), BF16),
            pltpu.VMEM((channels, width), BF16),
            pltpu.VMEM((16, rows), F32),
            pltpu.VMEM(((count - 1) * share + capacity, rows), BF16),
            pltpu.VMEM((count - 1, share, width), BF16),
            pltpu.VMEM((count, 4, share, width), BF16),
            pltpu.VMEM((4 * capacity, ff), BF16),
            pltpu.VMEM((count, 4, capacity, quarter), BF16),
        ]
        + [chunk] * 6
        + [
            pltpu.VMEM((rows, count * capacity), BF16),
            pltpu.VMEM((rows, count * capacity), BF16),
            pltpu.VMEM((4, rows, quarter), BF16),
            pltpu.VMEM((rows + 32, channels), BF16),
            pltpu.VMEM((rows + 32, channels), F32),
            pltpu.VMEM((rows, channels), BF16),
            pltpu.VMEM((rows, width), BF16),
            dma((2 * tiles + 11,)),
            dma((4, count)),
            dma((4, count)),
            dma((4, count)),
            dma((4, count)),
            dma((2, 7)),
            dma((2, 7)),
            dma((2,)),
            dma((2,)),
            dma((3, 2)),
            dma((3, 2)),
            dma((5,)),
        ],
        compiler_params=pltpu.CompilerParams(
            collective_id=0, has_side_effects=True, vmem_limit_bytes=VMEM_LIMIT
        ),
        cost_estimate=pl.CostEstimate(flops=7 * 10**9, bytes_accessed=2**24, transcendentals=0),
        name="layer",
    )(*operands)


def per_device(*operands):
    if lax.axis_size("tp") == 4 and lax.axis_size("ep") == 8:
        return fused(*operands)
    return mixer_half(*operands[:6]), expert_half(*operands[6:])


def solution(mesh):
    placed = (
        P(("ep", "tp"), None),
        P(),
        P(None, "tp"),
        P(),
        P(),
        P("tp", None),
        P("ep", None),
        P(),
        P("ep", None),
        P("ep", None),
        P("ep", None, "tp"),
        P("ep", None, "tp"),
        P("ep", "tp", None),
    )
    return jax.shard_map(
        per_device,
        mesh=mesh,
        in_specs=placed,
        out_specs=(P(("ep", "tp"), None), P("ep", None)),
        check_vma=False,
    )
```

time: 113 us -> 66.6 us (0.59)
  the two profiles are of different devices: /device:TPU:11 before, /device:TPU:1 now
where the time goes in v1:
time: 66.6 us; the launch traced here: 65.5 us
  Pallas kernels  61.1 us (92%)
  local copies, waits for them, and re-layouts  3.76 us (6%)
    pallas_call x1, Pallas kernels, fused(): pl.pallas_call(layer_kernel, out_shape=(jax.ShapeDtypeStruct(first_batch....  61.1 us
    unnamed x2, local copies, waits for them, and re-layouts  3.76 us

profile of v1, /device:TPU:1, one launch (start us, length us, event | category | flops | bytes accessed | tf_op | source)
XLA Modules:
  0.0 65.5 jit_solution(3222393580210396664)
XLA Ops:
  0.6 61.1 %layer.1 = (bf16[128,2048]{1,0:T(8,128)(2,1)}, bf16[128,2048]{1,0:T(8,128)(2,1)}) custom-call(bf16[128,2048]{1,0:T(8,128)(2,1)} %first_hbm.1, f32[1,2048]{1,0:T(1,128)} %bitcast.7, bf16[2048,128]{1,0:T(8,128)(2,1)} %mixer_in_hbm.1, bf16[512,64]{1,0:T(8,128)(2,1)} %bitcast.6, f32[1,512]{1,0:T(1,128)} %bitcast.9, bf16[128,2048]{1,0:T(8,128)(2,1)} %mixer_out_hbm.1, ...), custom_call_target="tpu_custom_call" | custom-call | flops 7000000000 | bytes 16777216 | tf_op jit(solution)/shard_map/layer/pallas_call | solution.py:647
  61.7 1.9 %copy.17 = bf16[128,2048]{1,0:T(8,128)(2,1)} copy(bf16[128,2048]{1,0:T(8,128)(2,1)} %get-tuple-element.4) | data formatting | bytes 1048576
  63.6 1.9 %copy.18 = bf16[128,2048]{1,0:T(8,128)(2,1)} copy(bf16[128,2048]{1,0:T(8,128)(2,1)} %get-tuple-element.5) | data formatting | bytes 1048576

commit v2 on v1

--- a/solution.py
+++ b/solution.py
@@ -140,16 +140,6 @@
     return place
 
 
-def weave(main, extra):
-    taken = 0
-    for i, step in enumerate(main):
-        step()
-        due = (i + 1) * len(extra) // len(main)
-        while taken < due:
-            extra[taken]()
-            taken += 1
-
-
 def normalize(source, gain, target):
     for i in range(0, source.shape[0], 16):
         floats = source[i : i + 16].astype(F32)
@@ -160,13 +150,13 @@
 def layer_kernel(
     first_hbm, mixer_gain_hbm, mixer_in_hbm, maps_hbm, scale_hbm, mixer_out_hbm,
     second_hbm, expert_gain_hbm, choice_hbm, scores_hbm, gate_hbm, up_hbm, down_hbm,
-    mixed_hbm, result_hbm,
+    mixed, result,
     x1, x2, n1, n2, gain1, gain2, scale, choice, scores, maps,
     w_in, w_down, m1, m2,
     rank_of, pick, portion, landed, hidden, part,
     side_y, side_own, sums_y, from_y, sums, slots, high, low, pieces,
-    padded, floats, grouped, mixed,
-    load, d_send, d_recv, c_send, c_recv, m_send, m_recv, h_send, h_recv, f_send, f_recv, store,
+    padded, floats, grouped,
+    load, d_send, d_recv, c_send, c_recv, m_send, m_recv, h_send, h_recv, f_send, f_recv,
 ):
     row, col = lax.axis_index("ep"), lax.axis_index("tp")
     count = landed.shape[0]
@@ -186,6 +176,8 @@
     peer = [(flip(row, k), col) for k in range(count)]
     on_chip, over_y = (row, partner), (row, across)
 
+    at = {k: i for i, k in enumerate(ORDER)}
+
     def remote(source, target, send, recv, device):
         return pltpu.make_async_remote_copy(
             src_ref=source, dst_ref=target, send_sem=send, recv_sem=recv,
@@ -237,11 +229,16 @@
         return rank_of[pl.ds(peer[k][0], 1), :]
 
     place = lax.broadcasted_iota(jnp.int32, (capacity, rows), 0).astype(F32)
+    core = col % 2
     offset = (col * share).astype(F32)
-    for k in range(1, count):
+    for k in range(2, count):
         chosen = place[:share] + offset == rank_at(k)
-        pick[(k - 1) * share : k * share] = chosen.astype(F32).astype(BF16)
-    own = (count - 1) * share
+        pick[(k - 2) * share : (k - 1) * share] = chosen.astype(F32).astype(BF16)
+    far = (count - 2) * share
+    pair = (core * 2 * share).astype(F32)
+    chosen = place[: 2 * share] + pair == rank_at(1)
+    pick[far : far + 2 * share] = chosen.astype(F32).astype(BF16)
+    own = far + 2 * share
     pick[own:] = (place == rank_at(0)).astype(F32).astype(BF16)
 
     loads["x2"].wait()
@@ -249,39 +246,40 @@
     normalize(x2, gain2, n2)
     for n in range(0, width, 256):
         taken = jnp.dot(pick[...], n2[:, n : n + 256], preferred_element_type=F32).astype(BF16)
-        portion[:, :, n : n + 256] = taken[:own].reshape(count - 1, share, 256)
-        landed[0, :, :, n : n + 256] = taken[own:].reshape(4, share, 256)
+        portion[:, :, n : n + 256] = taken[:own].reshape(count, share, 256)
+        landed[at[0], :, :, n : n + 256] = taken[own:].reshape(4, share, 256)
 
     loads["m1"].wait()
     loads["m2"].wait()
     pl.semaphore_wait(barrier, len(peers))
 
     firsts, ys, sides, corners = {}, {}, {}, {}
+    halves = landed.at[at[1], pl.ds(2 * core, 2)]
     for k in FIRST_ORDER:
-        firsts[k] = remote(
-            portion.at[k - 1], landed.at[k, col], d_send.at[0, k], d_recv.at[0, k], peer[k]
-        )
+        if k == 1:
+            source, target = portion.at[pl.ds(count - 2, 2)], halves
+        else:
+            source, target = portion.at[k - 2], landed.at[at[k], col]
+        firsts[k] = remote(source, target, d_send.at[0, k], d_recv.at[0, k], peer[k])
         firsts[k].start()
 
     def forward(k):
-        def run():
-            firsts[k].wait_recv()
-            block = landed.at[k, col]
-            ys[k] = remote(block, block, d_send.at[1, k], d_recv.at[1, k], over_y)
-            ys[k].start()
-            sides[k] = remote(block, block, d_send.at[2, k], d_recv.at[2, k], on_chip)
+        firsts[k].wait_recv()
+        if k == 1:
+            sides[k] = remote(halves, halves, d_send.at[2, k], d_recv.at[2, k], on_chip)
             sides[k].start()
-
-        return run
+            return
+        block = landed.at[at[k], col]
+        ys[k] = remote(block, block, d_send.at[1, k], d_recv.at[1, k], over_y)
+        ys[k].start()
+        sides[k] = remote(block, block, d_send.at[2, k], d_recv.at[2, k], on_chip)
+        sides[k].start()
 
     def turn(k):
-        def run():
-            ys[k].wait_recv()
-            block = landed.at[k, across]
-            corners[k] = remote(block, block, d_send.at[3, k], d_recv.at[3, k], on_chip)
-            corners[k].start()
-
-        return run
+        ys[k].wait_recv()
+        block = landed.at[at[k], across]
+        corners[k] = remote(block, block, d_send.at[3, k], d_recv.at[3, k], on_chip)
+        corners[k].start()
 
     fourth = row % 4
     moves = []
@@ -307,28 +305,19 @@
         own_shard[w] = move(w, 1, col, 0, 4, on_chip)
 
     def spread_x(w):
-        def run():
-            by_y[w].wait_recv()
-            by_x[w] = move(w, 2, across, fourth, 1, peer[1])
-            pass_y[w] = move(w, 3, across, fourth, 1, on_chip)
-
-        return run
+        by_y[w].wait_recv()
+        by_x[w] = move(w, 2, across, fourth, 1, peer[1])
+        pass_y[w] = move(w, 3, across, fourth, 1, on_chip)
 
     def spread_z(w):
-        def run():
-            by_x[w].wait_recv()
-            other = fourth + 1 - 2 * (fourth % 2)
-            by_z[w] = move(w, 4, across, 2 * (fourth // 2), 2, peer[2])
-            pass_x[w] = move(w, 5, across, other, 1, on_chip)
-
-        return run
+        by_x[w].wait_recv()
+        other = fourth + 1 - 2 * (fourth % 2)
+        by_z[w] = move(w, 4, across, 2 * (fourth // 2), 2, peer[2])
+        pass_x[w] = move(w, 5, across, other, 1, on_chip)
 
     def pass_on(w):
-        def run():
-            by_z[w].wait_recv()
-            pass_z[w] = move(w, 6, across, 2 - 2 * (fourth // 2), 2, on_chip)
-
-        return run
+        by_z[w].wait_recv()
+        pass_z[w] = move(w, 6, across, 2 - 2 * (fourth // 2), 2, on_chip)
 
     def gathered(w):
         for copy in (own_shard[w], pass_y[w], pass_x[w], pass_z[w]):
@@ -339,7 +328,7 @@
         weight_first = jax.nn.sigmoid(scores[0:1] - scores[1:2])
         for k in range(0, count, 2):
             blocks = []
-            for i in (k, k + 1):
+            for i in ORDER[k : k + 2]:
                 weight = jnp.where(first == peer[i][0], weight_first, 1.0 - weight_first)
                 blocks.append(jnp.where(place == rank_at(i), weight, 0.0))
             table = jnp.concatenate(blocks, axis=0).T
@@ -349,12 +338,11 @@
             low[:, columns] = (table - top.astype(F32)).astype(BF16)
 
     def arrive(start, stop):
-        def run():
-            for k in range(max(start, 1), stop):
+        for k in ORDER[start:stop]:
+            if k:
                 sides[k].wait_recv()
+            if k > 1:
                 corners[k].wait_recv()
-
-        return run
 
     weights_ready = set()
 
@@ -365,84 +353,75 @@
 
     to_side, to_own, to_y, to_ep = {}, {}, {}, {}
 
-    def expert_steps(start, stop):
+    def raise_up(start, stop):
         size = (stop - start) * capacity
-
-        def up(j):
-            def run():
-                ready(f"gate{j}")
-                ready(f"up{j}")
-                both = jnp.dot(
-                    landed[start:stop].reshape(size, width), w_in[j], preferred_element_type=F32
+        for j in range(tiles):
+            ready(f"gate{j}")
+            ready(f"up{j}")
+        for j in range(tiles):
+            both = jnp.dot(
+                landed[start:stop].reshape(size, width), w_in[j], preferred_element_type=F32
+            )
+            gate = both[:, :128]
+            hidden[:size, 128 * j : 128 * j + 128] = (
+                gate / (1.0 + jnp.exp(-gate)) * both[:, 128:]
+            ).astype(BF16)
+
+    def lower(start, stop, chosen):
+        ready("down")
+        size = (stop - start) * capacity
+        for i in chosen:
+            which = (corner, partner, across, col)[i]
+            for h in range(0, quarter, 256):
+                columns = pl.ds(pl.multiple_of(which * quarter + h, 256), 256)
+                part[start:stop, i, :, h : h + 256] = (
+                    jnp.dot(hidden[:size], w_down[:, columns], preferred_element_type=F32)
+                    .astype(BF16)
+                    .reshape(stop - start, capacity, 256)
                 )
-                gate = both[:, :128]
-                hidden[:size, 128 * j : 128 * j + 128] = (
-                    gate / (1.0 + jnp.exp(-gate)) * both[:, 128:]
-                ).astype(BF16)
-
-            return run
-
-        def down(i, which):
-            def run():
-                ready("down")
-                for h in range(0, quarter, 256):
-                    columns = pl.ds(pl.multiple_of(which * quarter + h, 256), 256)
-                    part[start:stop, i, :, h : h + 256] = (
-                        jnp.dot(hidden[:size], w_down[:, columns], preferred_element_type=F32)
-                        .astype(BF16)
-                        .reshape(stop - start, capacity, 256)
-                    )
-                for k in range(start, stop):
-                    if i == 1:
-                        to_side[k] = remote(
-                            part.at[k, 0], side_y.at[k], c_send.at[0, k], c_recv.at[0, k], on_chip
-                        )
-                        to_side[k].start()
-                    if i == 2:
-                        to_own[k] = remote(
-                            part.at[k, 1], side_own.at[k], c_send.at[1, k], c_recv.at[1, k], on_chip
-                        )
-                        to_own[k].start()
-
-            return run
-
-        return [up(j) for j in range(tiles)] + [
-            down(i, q) for i, q in enumerate((corner, partner, across, col))
-        ]
-
-    def add_y(ks):
-        def run():
-            for k in ks:
-                to_side[k].wait_recv()
-                sums_y[k] = (part[k, 2].astype(F32) + side_y[k].astype(F32)).astype(BF16)
-            for k in ks:
-                to_y[k] = remote(
-                    sums_y.at[k], from_y.at[k], c_send.at[2, k], c_recv.at[2, k], over_y
-                )
-                to_y[k].start()
-
-        return run
-
-    def add_all(ks):
-        def run():
-            for k in ks:
-                to_own[k].wait_recv()
-                to_y[k].wait_recv()
-                total = (
-                    part[k, 3].astype(F32) + side_own[k].astype(F32) + from_y[k].astype(F32)
-                ).astype(BF16)
-                if k:
-                    sums[k] = total
-                else:
-                    slots[0] = total
-            for k in ks:
-                if k:
-                    to_ep[k] = remote(
-                        sums.at[k], slots.at[k], c_send.at[3, k], c_recv.at[3, k], peer[k]
-                    )
-                    to_ep[k].start()
-
-        return run
+
+    def share_part(start, stop):
+        for i, k in enumerate(ORDER[start:stop], start):
+            to_side[k] = remote(
+                part.at[i, 0], side_y.at[i], c_send.at[0, k], c_recv.at[0, k], on_chip
+            )
+            to_side[k].start()
+        for i, k in enumerate(ORDER[start:stop], start):
+            to_own[k] = remote(
+                part.at[i, 1], side_own.at[i], c_send.at[1, k], c_recv.at[1, k], on_chip
+            )
+            to_own[k].start()
+
+    def expert(start, stop, between=()):
+        raise_up(start, stop)
+        for step in between:
+            step()
+        lower(start, stop, (0, 1))
+        share_part(start, stop)
+        lower(start, stop, (2, 3))
+
+    def add_y(*ks):
+        for k in ks:
+            i = at[k]
+            to_side[k].wait_recv()
+            sums_y[i] = (part[i, 2].astype(F32) + side_y[i].astype(F32)).astype(BF16)
+            to_y[k] = remote(sums_y.at[i], from_y.at[i], c_send.at[2, k], c_recv.at[2, k], over_y)
+            to_y[k].start()
+
+    def add_all(*ks):
+        for k in ks:
+            i = at[k]
+            to_own[k].wait_recv()
+            to_y[k].wait_recv()
+            total = (
+                part[i, 3].astype(F32) + side_own[i].astype(F32) + from_y[i].astype(F32)
+            ).astype(BF16)
+            if k == 0:
+                slots[i] = total
+                continue
+            sums[i] = total
+            to_ep[k] = remote(sums.at[i], slots.at[i], c_send.at[3, k], c_recv.at[3, k], peer[k])
+            to_ep[k].start()
 
     halo = {}
 
@@ -517,21 +496,46 @@
                 grouped[...], m2[:, n : n + 256], preferred_element_type=F32
             ).astype(BF16)
 
-    stores = []
-
-    def keep(source, target):
-        copy = pltpu.make_async_copy(source, target, store.at[len(stores)])
-        copy.start()
-        stores.append(copy)
-
-    run_schedule(
-        forward, turn, spread_x, spread_z, pass_on, make_table, arrive, expert_steps, add_y,
-        add_all, mix_norm, mix_in, mix_edges, mix_centre, mix_out,
-        lambda: keep(mixed, mixed_hbm),
-    )
-
-    for k in EP_ORDER:
-        to_ep[k].wait_recv()
+    make_table()
+    mix_norm()
+    forward(2)
+    forward(1)
+    arrive(0, 2)
+    expert(0, 2, [lambda: forward(4)])
+    forward(3)
+    spread_x(0)
+    spread_x(1)
+    turn(2)
+    forward(5)
+    turn(4)
+    forward(6)
+    add_y(1)
+    arrive(2, 4)
+    expert(2, 4, [lambda: turn(3), lambda: forward(7)])
+    spread_z(0)
+    add_y(4, 2)
+    turn(5)
+    add_all(1)
+    arrive(4, 6)
+    expert(4, 6, [lambda: turn(6)])
+    add_y(5)
+    turn(7)
+    add_all(4)
+    arrive(6, 8)
+    expert(6, 8, [lambda: add_all(2)])
+    add_y(7, 6, 3, 0)
+    add_all(5)
+    pass_on(0)
+    mix_in()
+    mix_edges()
+    add_all(7, 6, 3)
+    spread_z(1)
+    add_all(0)
+    mix_centre()
+
+    for k in ORDER:
+        if k:
+            to_ep[k].wait_recv()
     half = rows // 2
     out_y, out_side, out_corner = {}, {}, {}
     for h in range(2):
@@ -550,22 +554,25 @@
         out_side[h] = remote(block, block, f_send.at[1, h], f_recv.at[1, h], on_chip)
         out_side[h].start()
 
-    def quarter_of(which):
-        return result_hbm.at[:, pl.ds(pl.multiple_of(which * quarter, quarter), quarter)]
-
-    keep(pieces.at[col], quarter_of(col))
+    def place_piece(which):
+        columns = pl.ds(pl.multiple_of(which * quarter, quarter), quarter)
+        result[:, columns] = pieces[which]
+
+    place_piece(col)
     for h in range(2):
         out_y[h].wait_recv()
         block = pieces.at[across, pl.ds(h * half, half)]
         out_corner[h] = remote(block, block, f_send.at[2, h], f_recv.at[2, h], on_chip)
         out_corner[h].start()
-    keep(pieces.at[across], quarter_of(across))
+    place_piece(across)
+    pass_on(1)
+    mix_out()
     for h in range(2):
         out_side[h].wait_recv()
-    keep(pieces.at[partner], quarter_of(partner))
+    place_piece(partner)
     for h in range(2):
         out_corner[h].wait_recv()
-    keep(pieces.at[corner], quarter_of(corner))
+    place_piece(corner)
 
     for k in range(count):
         to_side[k].wait_send()
@@ -573,10 +580,11 @@
         to_y[k].wait_send()
         if k:
             firsts[k].wait_send()
+            sides[k].wait_send()
+            to_ep[k].wait_send()
+        if k > 1:
             ys[k].wait_send()
-            sides[k].wait_send()
             corners[k].wait_send()
-            to_ep[k].wait_send()
     for copy in moves:
         copy.wait_send()
     for i in range(2):
@@ -584,43 +592,46 @@
         out_y[i].wait_send()
         out_side[i].wait_send()
         out_corner[i].wait_send()
+
+
+FIRST_ORDER = (1, 4, 5, 2, 3, 6, 7)
+ORDER = (1, 0, 4, 2, 5, 3, 6, 7)
+
+
+def finish_kernel(mixed, result, mixed_out, result_out, held, into, out):
+    step = held.shape[1] // 4
+    loads, stores = [], []
+    for i, source in enumerate((result, mixed)):
+        for j in range(4):
+            rows = pl.ds(step * j, step)
+            copy = pltpu.make_async_copy(source.at[rows], held.at[i, rows], into.at[4 * i + j])
+            copy.start()
+            loads.append(copy)
+    for i, target in enumerate((result_out, mixed_out)):
+        for j in range(4):
+            rows = pl.ds(step * j, step)
+            loads[4 * i + j].wait()
+            copy = pltpu.make_async_copy(held.at[i, rows], target.at[rows], out.at[4 * i + j])
+            copy.start()
+            stores.append(copy)
     for copy in stores:
         copy.wait()
 
 
-FIRST_ORDER = (4, 5, 1, 2, 3, 6, 7)
-EP_ORDER = (1, 2, 3, 4, 5, 6, 7)
-
-
-def run_schedule(
-    forward, turn, spread_x, spread_z, pass_on, make_table, arrive, expert_steps, add_y,
-    add_all, mix_norm, mix_in, mix_edges, mix_centre, mix_out, keep_mixed,
-):
-    make_table()
-    mix_norm()
-    for step in (forward(1), forward(4), forward(2), turn(1), forward(3), spread_x(0)):
-        step()
-    arrive(0, 2)()
-    weave(expert_steps(0, 2), [turn(2), forward(5), turn(3), spread_x(1)])
-    arrive(2, 4)()
-    weave(expert_steps(2, 4), [turn(4), add_y((1, 0)), forward(6), turn(5)])
-    arrive(4, 6)()
-    weave(
-        expert_steps(4, 6),
-        [add_y((2, 3)), forward(7), turn(6), add_all((1, 0)), spread_z(0), spread_z(1), turn(7)],
-    )
-    arrive(6, 8)()
-    weave(expert_steps(6, 8), [add_y((4, 5)), add_all((2, 3))])
-    add_all((4, 5))()
-    add_y((6, 7))()
-    pass_on(0)()
-    add_all((6, 7))()
-    mix_in()
-    mix_edges()
-    pass_on(1)()
-    mix_centre()
-    mix_out()
-    keep_mixed()
+def finish(mixed, result):
+    anywhere = pl.BlockSpec(memory_space=pl.ANY)
+    return pl.pallas_call(
+        finish_kernel,
+        out_shape=tuple(jax.ShapeDtypeStruct(x.shape, x.dtype) for x in (mixed, result)),
+        in_specs=[anywhere] * 2,
+        out_specs=(anywhere, anywhere),
+        scratch_shapes=[
+            pltpu.VMEM((2,) + result.shape, result.dtype),
+            pltpu.SemaphoreType.DMA((8,)),
+            pltpu.SemaphoreType.DMA((8,)),
+        ],
+        name="finish",
+    )(mixed, result)
 
 
 def fused(
@@ -637,21 +648,22 @@
     tiles = ff // 128
     chunk = pltpu.VMEM((count, capacity, quarter), BF16)
     dma = pltpu.SemaphoreType.DMA
-    anywhere = pl.BlockSpec(memory_space=pl.ANY)
+    in_hbm = pl.BlockSpec(memory_space=pltpu.HBM)
+    in_vmem = pl.BlockSpec(memory_space=pltpu.VMEM)
     operands = (
         first_batch, mixer_gain.reshape(1, width), mixer_in,
         group_maps.reshape(channels, GROUP), pool_scale.reshape(1, channels), mixer_out,
         second_batch, expert_gain.reshape(1, width), expert_choice.T, route_scores.T,
         expert_gate, expert_up, expert_down,
     )
-    return pl.pallas_call(
+    return finish(*pl.pallas_call(
         layer_kernel,
         out_shape=(
             jax.ShapeDtypeStruct(first_batch.shape, BF16),
             jax.ShapeDtypeStruct(second_batch.shape, BF16),
         ),
-        in_specs=[anywhere] * len(operands),
-        out_specs=(anywhere, anywhere),
+        in_specs=[in_hbm] * len(operands),
+        out_specs=(in_vmem, in_vmem),
         scratch_shapes=[
             pltpu.VMEM((rows, width), BF16),
             pltpu.VMEM((rows, width), BF16),
@@ -668,8 +680,8 @@
             pltpu.VMEM((width, channels), BF16),
             pltpu.VMEM((channels, width), BF16),
             pltpu.VMEM((16, rows), F32),
-            pltpu.VMEM(((count - 1) * share + capacity, rows), BF16),
-            pltpu.VMEM((count - 1, share, width), BF16),
+            pltpu.VMEM((count * share + capacity, rows), BF16),
+            pltpu.VMEM((count, share, width), BF16),
             pltpu.VMEM((count, 4, share, width), BF16),
             pltpu.VMEM((4 * capacity, ff), BF16),
             pltpu.VMEM((count, 4, capacity, quarter), BF16),
@@ -682,7 +694,6 @@
             pltpu.VMEM((rows + 32, channels), BF16),
             pltpu.VMEM((rows + 32, channels), F32),
             pltpu.VMEM((rows, channels), BF16),
-            pltpu.VMEM((rows, width), BF16),
             dma((2 * tiles + 11,)),
             dma((4, count)),
             dma((4, count)),
@@ -694,14 +705,13 @@
             dma((2,)),
             dma((3, 2)),
             dma((3, 2)),
-            dma((5,)),
         ],
         compiler_params=pltpu.CompilerParams(
             collective_id=0, has_side_effects=True, vmem_limit_bytes=VMEM_LIMIT
         ),
         cost_estimate=pl.CostEstimate(flops=7 * 10**9, bytes_accessed=2**24, transcendentals=0),
         name="layer",
-    )(*operands)
+    )(*operands))
 
 
 def per_device(*operands):

time: 66.6 us -> 54 us (0.81); the launches traced: 65.5 us -> 53.9 us
  Pallas kernels: 61.1 us -> 53.2 us
  local copies, waits for them, and re-layouts: 3.76 us -> 0 us
    pallas_call x1, Pallas kernels: 61.1 us -> 51.2 us  [fused(): pl.pallas_call(layer_kernel, out_shape=(jax.ShapeDtypeStruct(first_batch....]
    unnamed x2 -> x0, local copies, waits for them, and re-layouts: 3.76 us -> none
    pallas_call x0 -> x1, Pallas kernels: none -> 2.09 us  [finish(): pl.pallas_call(finish_kernel, out_shape=tuple((jax.ShapeDtypeStruct(x.sha...]
where the time goes in v2:
time: 54 us; the launch traced here: 53.9 us
  Pallas kernels  53.2 us (99%)
  between operations  0.64 us (1%)
    pallas_call x1, Pallas kernels, fused(): pl.pallas_call(layer_kernel, out_shape=(jax.ShapeDtypeStruct(first_batch....  51.2 us
    pallas_call x1, Pallas kernels, finish(): pl.pallas_call(finish_kernel, out_shape=tuple((jax.ShapeDtypeStruct(x.sha...  2.09 us

profile of v2, /device:TPU:1, one launch (start us, length us, event | category | flops | bytes accessed | tf_op | source)
XLA Modules:
  0.0 53.9 jit_solution(8206762143507621407)
XLA Ops:
  0.6 51.2 %layer.1 = (bf16[128,2048]{1,0:T(8,128)(2,1)}, bf16[128,2048]{1,0:T(8,128)(2,1)}) custom-call(bf16[128,2048]{1,0:T(8,128)(2,1)} %first_hbm.1, f32[1,2048]{1,0:T(1,128)} %bitcast.7, bf16[2048,128]{1,0:T(8,128)(2,1)} %mixer_in_hbm.1, bf16[512,64]{1,0:T(8,128)(2,1)} %bitcast.6, f32[1,512]{1,0:T(1,128)} %bitcast.9, bf16[128,2048]{1,0:T(8,128)(2,1)} %mixer_out_hbm.1, ...), custom_call_target="tpu_custom_call" | custom-call | flops 7000000000 | bytes 16777216 | tf_op jit(solution)/shard_map/layer/pallas_call | solution.py:659
  51.8 2.1 %finish.1 = (bf16[128,2048]{1,0:T(8,128)(2,1)}, bf16[128,2048]{1,0:T(8,128)(2,1)}) custom-call(bf16[128,2048]{1,0:T(8,128)(2,1)} %get-tuple-element.4.mixed, bf16[128,2048]{1,0:T(8,128)(2,1)} %get-tuple-element.5.result), custom_call_target="tpu_custom_call" | custom-call | tf_op jit(solution)/shard_map/finish/pallas_call | solution.py:623

commit v3 on v2

--- a/solution.py
+++ b/solution.py
@@ -150,13 +150,14 @@
 def layer_kernel(
     first_hbm, mixer_gain_hbm, mixer_in_hbm, maps_hbm, scale_hbm, mixer_out_hbm,
     second_hbm, expert_gain_hbm, choice_hbm, scores_hbm, gate_hbm, up_hbm, down_hbm,
-    mixed, result,
+    mixed_hbm, result_hbm,
     x1, x2, n1, n2, gain1, gain2, scale, choice, scores, maps,
     w_in, w_down, m1, m2,
     rank_of, pick, portion, landed, hidden, part,
     side_y, side_own, sums_y, from_y, sums, slots, high, low, pieces,
-    padded, floats, grouped,
-    load, d_send, d_recv, c_send, c_recv, m_send, m_recv, h_send, h_recv, f_send, f_recv,
+    padded, floats, grouped, mixed,
+    load, d_send, first_recv, y_recv, block_recv, c_send, part_recv, sum_recv, slot_recv,
+    m_send, m_recv, h_send, h_recv, f_send, f_recv, store,
 ):
     row, col = lax.axis_index("ep"), lax.axis_index("tp")
     count = landed.shape[0]
@@ -203,10 +204,13 @@
     fetch("gain1", mixer_gain_hbm, gain1)
     fetch("maps", maps_hbm, maps)
     fetch("scale", scale_hbm, scale)
+    fetch("down", down_hbm.at[0], w_down)
+    sem = load.at[len(loads)]
     for j in range(tiles):
-        fetch(f"gate{j}", gate_hbm.at[0, :, pl.ds(128 * j, 128)], w_in.at[j, :, pl.ds(0, 128)])
-        fetch(f"up{j}", up_hbm.at[0, :, pl.ds(128 * j, 128)], w_in.at[j, :, pl.ds(128, 128)])
-    fetch("down", down_hbm.at[0], w_down)
+        for i, source in enumerate((gate_hbm, up_hbm)):
+            target = w_in.at[j, :, pl.ds(128 * i, 128)]
+            pltpu.make_async_copy(source.at[0, :, pl.ds(128 * j, 128)], target, sem).start()
+    loads["w_in"] = pltpu.make_async_copy(w_in, w_in, sem)
 
     barrier = pltpu.get_barrier_semaphore()
     peers = peer[1:] + [on_chip, over_y, after_device, before_device]
@@ -260,29 +264,28 @@
             source, target = portion.at[pl.ds(count - 2, 2)], halves
         else:
             source, target = portion.at[k - 2], landed.at[at[k], col]
-        firsts[k] = remote(source, target, d_send.at[0, k], d_recv.at[0, k], peer[k])
+        firsts[k] = remote(source, target, d_send.at[0], first_recv.at[k], peer[k])
         firsts[k].start()
 
     def forward(k):
         firsts[k].wait_recv()
         if k == 1:
-            sides[k] = remote(halves, halves, d_send.at[2, k], d_recv.at[2, k], on_chip)
+            sides[k] = remote(halves, halves, d_send.at[2], block_recv.at[at[k] // 2], on_chip)
             sides[k].start()
             return
         block = landed.at[at[k], col]
-        ys[k] = remote(block, block, d_send.at[1, k], d_recv.at[1, k], over_y)
+        ys[k] = remote(block, block, d_send.at[1], y_recv.at[k], over_y)
         ys[k].start()
-        sides[k] = remote(block, block, d_send.at[2, k], d_recv.at[2, k], on_chip)
+        sides[k] = remote(block, block, d_send.at[2], block_recv.at[at[k] // 2], on_chip)
         sides[k].start()
 
     def turn(k):
         ys[k].wait_recv()
         block = landed.at[at[k], across]
-        corners[k] = remote(block, block, d_send.at[3, k], d_recv.at[3, k], on_chip)
+        corners[k] = remote(block, block, d_send.at[3], block_recv.at[at[k] // 2], on_chip)
         corners[k].start()
 
-    fourth = row % 4
-    moves = []
+    fourth = (row % 2) * 2 + (row // 2) % 2
 
     def piece(which, owner, start, size):
         if which == 0:
@@ -293,35 +296,38 @@
 
     def move(which, kind, owner, start, size, device):
         block = piece(which, owner, start, size)
-        copy = remote(block, block, m_send.at[which, kind], m_recv.at[which, kind], device)
+        copy = remote(block, block, m_send.at[which], m_recv.at[which, kind], device)
         copy.start()
-        moves.append(copy)
         return copy
 
-    own_shard, by_y, by_x, by_z, pass_y, pass_x, pass_z = {}, {}, {}, {}, {}, {}, {}
+    by_y, by_z, by_x = {}, {}, {}
     for w in range(2):
         by_y[w] = move(w, 0, col, fourth, 1, over_y)
     for w in range(2):
-        own_shard[w] = move(w, 1, col, 0, 4, on_chip)
+        move(w, 3, col, 0, 4, on_chip)
+
+    def spread_z(w):
+        by_y[w].wait_recv()
+        by_z[w] = move(w, 1, across, fourth, 1, peer[2])
+        move(w, 3, across, fourth, 1, on_chip)
 
     def spread_x(w):
-        by_y[w].wait_recv()
-        by_x[w] = move(w, 2, across, fourth, 1, peer[1])
-        pass_y[w] = move(w, 3, across, fourth, 1, on_chip)
-
-    def spread_z(w):
+        by_z[w].wait_recv()
+        other = fourth + 1 - 2 * (fourth % 2)
+        by_x[w] = move(w, 2, across, 2 * (fourth // 2), 2, peer[1])
+        move(w, 3, across, other, 1, on_chip)
+
+    def pass_on(w):
         by_x[w].wait_recv()
-        other = fourth + 1 - 2 * (fourth % 2)
-        by_z[w] = move(w, 4, across, 2 * (fourth // 2), 2, peer[2])
-        pass_x[w] = move(w, 5, across, other, 1, on_chip)
-
-    def pass_on(w):
-        by_z[w].wait_recv()
-        pass_z[w] = move(w, 6, across, 2 - 2 * (fourth // 2), 2, on_chip)
+        move(w, 3, across, 2 - 2 * (fourth // 2), 2, on_chip)
+
+    def whole(which, parts):
+        ref = (m1, m2)[which]
+        block = ref.at[pl.ds(0, ref.shape[0] * parts // 4)]
+        return remote(block, block, m_send.at[which], m_recv.at[which, 3], on_chip)
 
     def gathered(w):
-        for copy in (own_shard[w], pass_y[w], pass_x[w], pass_z[w]):
-            copy.wait_recv()
+        whole(w, 2).wait_recv()
 
     def make_table():
         loads["scores"].wait()
@@ -337,12 +343,10 @@
             high[:, columns] = top
             low[:, columns] = (table - top.astype(F32)).astype(BF16)
 
-    def arrive(start, stop):
-        for k in ORDER[start:stop]:
-            if k:
-                sides[k].wait_recv()
-            if k > 1:
-                corners[k].wait_recv()
+    def arrive(chunk):
+        blocks = sum(2 for k in ORDER[2 * chunk : 2 * chunk + 2] if k)
+        landing = landed.at[2 * chunk, pl.ds(0, blocks)]
+        remote(landing, landing, d_send.at[2], block_recv.at[chunk], on_chip).wait_recv()
 
     weights_ready = set()
 
@@ -353,12 +357,10 @@
 
     to_side, to_own, to_y, to_ep = {}, {}, {}, {}
 
-    def raise_up(start, stop):
+    def raise_up(start, stop, chosen):
         size = (stop - start) * capacity
-        for j in range(tiles):
-            ready(f"gate{j}")
-            ready(f"up{j}")
-        for j in range(tiles):
+        ready("w_in")
+        for j in chosen:
             both = jnp.dot(
                 landed[start:stop].reshape(size, width), w_in[j], preferred_element_type=F32
             )
@@ -383,35 +385,46 @@
     def share_part(start, stop):
         for i, k in enumerate(ORDER[start:stop], start):
             to_side[k] = remote(
-                part.at[i, 0], side_y.at[i], c_send.at[0, k], c_recv.at[0, k], on_chip
+                part.at[i, 0], side_y.at[i], c_send.at[0], part_recv.at[i // 2], on_chip
             )
             to_side[k].start()
         for i, k in enumerate(ORDER[start:stop], start):
             to_own[k] = remote(
-                part.at[i, 1], side_own.at[i], c_send.at[1, k], c_recv.at[1, k], on_chip
+                part.at[i, 1], side_own.at[i], c_send.at[1], part_recv.at[i // 2], on_chip
             )
             to_own[k].start()
 
-    def expert(start, stop, between=()):
-        raise_up(start, stop)
+    def expert(start, stop, within=(), between=()):
+        middle = tiles // 2 if within else 0
+        raise_up(start, stop, range(middle))
+        for step in within:
+            step()
+        raise_up(start, stop, range(middle, tiles))
         for step in between:
             step()
         lower(start, stop, (0, 1))
         share_part(start, stop)
         lower(start, stop, (2, 3))
 
+    met = set()
+
+    def halved(chunk):
+        if chunk not in met:
+            met.add(chunk)
+            block = side_y.at[pl.ds(0, 4)]
+            remote(block, block, c_send.at[0], part_recv.at[chunk], on_chip).wait_recv()
+
     def add_y(*ks):
         for k in ks:
             i = at[k]
-            to_side[k].wait_recv()
+            halved(i // 2)
             sums_y[i] = (part[i, 2].astype(F32) + side_y[i].astype(F32)).astype(BF16)
-            to_y[k] = remote(sums_y.at[i], from_y.at[i], c_send.at[2, k], c_recv.at[2, k], over_y)
+            to_y[k] = remote(sums_y.at[i], from_y.at[i], c_send.at[2], sum_recv.at[k], over_y)
             to_y[k].start()
 
     def add_all(*ks):
         for k in ks:
             i = at[k]
-            to_own[k].wait_recv()
             to_y[k].wait_recv()
             total = (
                 part[i, 3].astype(F32) + side_own[i].astype(F32) + from_y[i].astype(F32)
@@ -420,7 +433,7 @@
                 slots[i] = total
                 continue
             sums[i] = total
-            to_ep[k] = remote(sums.at[i], slots.at[i], c_send.at[3, k], c_recv.at[3, k], peer[k])
+            to_ep[k] = remote(sums.at[i], slots.at[i], c_send.at[3], slot_recv.at[0], peer[k])
             to_ep[k].start()
 
     halo = {}
@@ -444,14 +457,17 @@
         )
         halo[0].start()
         halo[1] = remote(
-            padded.at[pl.ds(16, 16)], padded.at[pl.ds(16 + rows, 16)], h_send.at[1], h_recv.at[1],
+            padded.at[pl.ds(16, 16)], padded.at[pl.ds(16 + rows, 16)], h_send.at[0], h_recv.at[0],
             before_device,
         )
         halo[1].start()
 
+    def both_edges():
+        edges = padded.at[pl.ds(0, 32)]
+        return remote(edges, edges, h_send.at[0], h_recv.at[0], after_device)
+
     def mix_centre():
-        halo[0].wait_recv()
-        halo[1].wait_recv()
+        both_edges().wait_recv()
         loads["maps"].wait()
         loads["scale"].wait()
         seq_length = rows * devices // SEQS
@@ -498,104 +514,90 @@
 
     make_table()
     mix_norm()
+    spread_z(0)
+    forward(4)
     forward(2)
     forward(1)
-    arrive(0, 2)
-    expert(0, 2, [lambda: forward(4)])
     forward(3)
+    spread_z(1)
+    turn(4)
+    forward(5)
+    arrive(0)
+    expert(0, 2, between=[lambda: forward(6), lambda: turn(2)])
+    turn(3)
+    forward(7)
     spread_x(0)
+    add_y(4)
+    turn(5)
+    arrive(1)
+    expert(2, 4, between=[lambda: turn(6)])
     spread_x(1)
-    turn(2)
-    forward(5)
-    turn(4)
-    forward(6)
-    add_y(1)
-    arrive(2, 4)
-    expert(2, 4, [lambda: turn(3), lambda: forward(7)])
-    spread_z(0)
-    add_y(4, 2)
-    turn(5)
+    arrive(2)
+    expert(4, 6, [lambda: add_y(5, 1), lambda: add_all(4)], [lambda: turn(7)])
+    arrive(3)
+    expert(6, 8, [lambda: add_y(6, 3)], [lambda: add_all(5)])
     add_all(1)
-    arrive(4, 6)
-    expert(4, 6, [lambda: turn(6)])
-    add_y(5)
-    turn(7)
-    add_all(4)
-    arrive(6, 8)
-    expert(6, 8, [lambda: add_all(2)])
-    add_y(7, 6, 3, 0)
-    add_all(5)
+    add_y(7, 2, 0)
+    add_all(6)
     pass_on(0)
     mix_in()
     mix_edges()
-    add_all(7, 6, 3)
-    spread_z(1)
-    add_all(0)
+    add_all(3, 7, 2, 0)
     mix_centre()
-
-    for k in ORDER:
-        if k:
-            to_ep[k].wait_recv()
-    half = rows // 2
-    out_y, out_side, out_corner = {}, {}, {}
-    for h in range(2):
-        held = slice(h * half, h * half + half)
-        returned = slots[...].reshape(count * capacity, quarter)
-        pieces[col, held] = (
-            jnp.dot(high[held], returned, preferred_element_type=F32)
-            + jnp.dot(low[held], returned, preferred_element_type=F32)
-        ).astype(BF16)
-    for h in range(2):
-        block = pieces.at[col, pl.ds(h * half, half)]
-        out_y[h] = remote(block, block, f_send.at[0, h], f_recv.at[0, h], over_y)
+    pass_on(1)
+
+    back = slots.at[pl.ds(0, count - 1)]
+    remote(back, back, c_send.at[3], slot_recv.at[0], on_chip).wait_recv()
+    bits = rows // 4
+    out_y = {}
+    returned = slots[...].reshape(count * capacity, quarter)
+    pieces[col] = (
+        jnp.dot(high[...], returned, preferred_element_type=F32)
+        + jnp.dot(low[...], returned, preferred_element_type=F32)
+    ).astype(BF16)
+    for h in range(4):
+        block = pieces.at[col, pl.ds(h * bits, bits)]
+        out_y[h] = remote(block, block, f_send.at[0], f_recv.at[h], over_y)
         out_y[h].start()
-    for h in range(2):
-        block = pieces.at[col, pl.ds(h * half, half)]
-        out_side[h] = remote(block, block, f_send.at[1, h], f_recv.at[1, h], on_chip)
-        out_side[h].start()
+    own_piece = pieces.at[col]
+    out_side = remote(own_piece, own_piece, f_send.at[0], f_recv.at[4], on_chip)
+    out_side.start()
 
     def place_piece(which):
         columns = pl.ds(pl.multiple_of(which * quarter, quarter), quarter)
-        result[:, columns] = pieces[which]
+        pltpu.make_async_copy(pieces.at[which], result_hbm.at[:, columns], store.at[0]).start()
 
     place_piece(col)
-    for h in range(2):
+    for h in range(4):
         out_y[h].wait_recv()
-        block = pieces.at[across, pl.ds(h * half, half)]
-        out_corner[h] = remote(block, block, f_send.at[2, h], f_recv.at[2, h], on_chip)
-        out_corner[h].start()
+        block = pieces.at[across, pl.ds(h * bits, bits)]
+        remote(block, block, f_send.at[0], f_recv.at[5], on_chip).start()
     place_piece(across)
-    pass_on(1)
+    out_side.wait_recv()
+    place_piece(partner)
     mix_out()
-    for h in range(2):
-        out_side[h].wait_recv()
-    place_piece(partner)
-    for h in range(2):
-        out_corner[h].wait_recv()
+    mixed_store = pltpu.make_async_copy(mixed, mixed_hbm, store.at[1])
+    mixed_store.start()
+    other_piece = pieces.at[corner]
+    remote(other_piece, other_piece, f_send.at[0], f_recv.at[5], on_chip).wait_recv()
     place_piece(corner)
 
-    for k in range(count):
-        to_side[k].wait_send()
-        to_own[k].wait_send()
-        to_y[k].wait_send()
-        if k:
-            firsts[k].wait_send()
-            sides[k].wait_send()
-            to_ep[k].wait_send()
-        if k > 1:
-            ys[k].wait_send()
-            corners[k].wait_send()
-    for copy in moves:
-        copy.wait_send()
-    for i in range(2):
-        halo[i].wait_send()
-        out_y[i].wait_send()
-        out_side[i].wait_send()
-        out_corner[i].wait_send()
+    full, six = portion.at[pl.ds(0, count)], portion.at[pl.ds(0, count - 2)]
+    for i, block in enumerate((full, six, full, six)):
+        remote(block, block, d_send.at[i], first_recv.at[0], on_chip).wait_send()
+    for i, block in enumerate((slots, slots, slots, back)):
+        remote(block, block, c_send.at[i], slot_recv.at[0], on_chip).wait_send()
+    for w in range(2):
+        whole(w, 3).wait_send()
+    both_edges().wait_send()
+    three = pieces.at[pl.ds(0, 3)]
+    remote(three, three, f_send.at[0], f_recv.at[5], on_chip).wait_send()
+    mixed_store.wait()
+    pltpu.make_async_copy(mixed, result_hbm, store.at[0]).wait()
 
 
 FIRST_ORDER = (1, 4, 5, 2, 3, 6, 7)
-ORDER = (1, 0, 4, 2, 5, 3, 6, 7)
+ORDER = (1, 4, 5, 2, 6, 3, 7, 0)
 
 
 def finish_kernel(mixed, result, mixed_out, result_out, held, into, out):
@@ -649,7 +651,6 @@
     chunk = pltpu.VMEM((count, capacity, quarter), BF16)
     dma = pltpu.SemaphoreType.DMA
     in_hbm = pl.BlockSpec(memory_space=pltpu.HBM)
-    in_vmem = pl.BlockSpec(memory_space=pltpu.VMEM)
     operands = (
         first_batch, mixer_gain.reshape(1, width), mixer_in,
         group_maps.reshape(channels, GROUP), pool_scale.reshape(1, channels), mixer_out,
@@ -663,7 +664,7 @@
             jax.ShapeDtypeStruct(second_batch.shape, BF16),
         ),
         in_specs=[in_hbm] * len(operands),
-        out_specs=(in_vmem, in_vmem),
+        out_specs=(in_hbm, in_hbm),
         scratch_shapes=[
             pltpu.VMEM((rows, width), BF16),
             pltpu.VMEM((rows, width), BF16),
@@ -694,17 +695,23 @@
             pltpu.VMEM((rows + 32, channels), BF16),
             pltpu.VMEM((rows + 32, channels), F32),
             pltpu.VMEM((rows, channels), BF16),
-            dma((2 * tiles + 11,)),
-            dma((4, count)),
-            dma((4, count)),
-            dma((4, count)),
-            dma((4, count)),
-            dma((2, 7)),
-            dma((2, 7)),
+            pltpu.VMEM((rows, width), BF16),
+            dma((12,)),
+            dma((4,)),
+            dma((count,)),
+            dma((count,)),
+            dma((count // 2,)),
+            dma((4,)),
+            dma((count // 2,)),
+            dma((count,)),
+            dma((1,)),
             dma((2,)),
+            dma((2, 4)),
+            dma((1,)),
+            dma((1,)),
+            dma((1,)),
+            dma((6,)),
             dma((2,)),
-            dma((3, 2)),
-            dma((3, 2)),
         ],
         compiler_params=pltpu.CompilerParams(
             collective_id=0, has_side_effects=True, vmem_limit_bytes=VMEM_LIMIT

time: 54 us -> 50.2 us (0.930)
  Pallas kernels: 53.2 us -> 49.5 us
    pallas_call x1, Pallas kernels: 51.2 us -> 47.4 us  [fused(): pl.pallas_call(layer_kernel, out_shape=(jax.ShapeDtypeStruct(first_batch....]
where the time goes in v3:
time: 50.2 us; the launch traced here: 50.1 us
  Pallas kernels  49.5 us (99%)
  between operations  0.64 us (1%)
    pallas_call x1, Pallas kernels, fused(): pl.pallas_call(layer_kernel, out_shape=(jax.ShapeDtypeStruct(first_batch....  47.4 us
    pallas_call x1, Pallas kernels, finish(): pl.pallas_call(finish_kernel, out_shape=tuple((jax.ShapeDtypeStruct(x.sha...  2.09 us

profile of v3, /device:TPU:1, one launch (start us, length us, event | category | flops | bytes accessed | tf_op | source)
XLA Modules:
  0.0 50.1 jit_solution(1430677294557080611)
XLA Ops:
  0.6 47.4 %layer.1 = (bf16[128,2048]{1,0:T(8,128)(2,1)}, bf16[128,2048]{1,0:T(8,128)(2,1)}) custom-call(bf16[128,2048]{1,0:T(8,128)(2,1)} %first_hbm.1, f32[1,2048]{1,0:T(1,128)} %bitcast.7, bf16[2048,128]{1,0:T(8,128)(2,1)} %mixer_in_hbm.1, bf16[512,64]{1,0:T(8,128)(2,1)} %bitcast.6, f32[1,512]{1,0:T(1,128)} %bitcast.9, bf16[128,2048]{1,0:T(8,128)(2,1)} %mixer_out_hbm.1, ...), custom_call_target="tpu_custom_call" | custom-call | flops 7000000000 | bytes 16777216 | tf_op jit(solution)/shard_map/layer/pallas_call | solution.py:660
  48.0 2.1 %finish.1 = (bf16[128,2048]{1,0:T(8,128)(2,1)}, bf16[128,2048]{1,0:T(8,128)(2,1)}) custom-call(bf16[128,2048]{1,0:T(8,128)(2,1)} %get-tuple-element.4.mixed, bf16[128,2048]{1,0:T(8,128)(2,1)} %get-tuple-element.5.result), custom_call_target="tpu_custom_call" | custom-call | tf_op jit(solution)/shard_map/finish/pallas_call | solution.py:625

commit v4 on v3

--- a/solution.py
+++ b/solution.py
@@ -204,13 +204,15 @@
     fetch("gain1", mixer_gain_hbm, gain1)
     fetch("maps", maps_hbm, maps)
     fetch("scale", scale_hbm, scale)
-    fetch("down", down_hbm.at[0], w_down)
-    sem = load.at[len(loads)]
-    for j in range(tiles):
-        for i, source in enumerate((gate_hbm, up_hbm)):
-            target = w_in.at[j, :, pl.ds(128 * i, 128)]
-            pltpu.make_async_copy(source.at[0, :, pl.ds(128 * j, 128)], target, sem).start()
-    loads["w_in"] = pltpu.make_async_copy(w_in, w_in, sem)
+
+    def fetch_weights():
+        sem = load.at[len(loads)]
+        for j in range(tiles):
+            for i, source in enumerate((gate_hbm, up_hbm)):
+                target = w_in.at[j, :, pl.ds(128 * i, 128)]
+                pltpu.make_async_copy(source.at[0, :, pl.ds(128 * j, 128)], target, sem).start()
+        loads["w_in"] = pltpu.make_async_copy(w_in, w_in, sem)
+        fetch("down", down_hbm.at[0], w_down)
 
     barrier = pltpu.get_barrier_semaphore()
     peers = peer[1:] + [on_chip, over_y, after_device, before_device]
@@ -512,6 +514,7 @@
                 grouped[...], m2[:, n : n + 256], preferred_element_type=F32
             ).astype(BF16)
 
+    fetch_weights()
     make_table()
     mix_norm()
     spread_z(0)
@@ -527,24 +530,29 @@
     turn(3)
     forward(7)
     spread_x(0)
-    add_y(4)
     turn(5)
+    add_y(4, 1)
     arrive(1)
     expert(2, 4, between=[lambda: turn(6)])
     spread_x(1)
     arrive(2)
-    expert(4, 6, [lambda: add_y(5, 1), lambda: add_all(4)], [lambda: turn(7)])
+    expert(4, 6, [lambda: add_y(5, 2)], [lambda: turn(7), lambda: add_all(4)])
     arrive(3)
-    expert(6, 8, [lambda: add_y(6, 3)], [lambda: add_all(5)])
-    add_all(1)
-    add_y(7, 2, 0)
+    expert(6, 8, [lambda: add_y(6)])
+    add_all(5, 1)
+    pass_on(0)
+    add_y(7, 3, 0)
     add_all(6)
-    pass_on(0)
     mix_in()
     mix_edges()
-    add_all(3, 7, 2, 0)
+    add_all(2)
+    add_all(7)
+    pass_on(1)
+    add_all(3, 0)
     mix_centre()
-    pass_on(1)
+    mix_out()
+    mixed_store = pltpu.make_async_copy(mixed, mixed_hbm, store.at[1])
+    mixed_store.start()
 
     back = slots.at[pl.ds(0, count - 1)]
     remote(back, back, c_send.at[3], slot_recv.at[0], on_chip).wait_recv()
@@ -575,9 +583,6 @@
     place_piece(across)
     out_side.wait_recv()
     place_piece(partner)
-    mix_out()
-    mixed_store = pltpu.make_async_copy(mixed, mixed_hbm, store.at[1])
-    mixed_store.start()
     other_piece = pieces.at[corner]
     remote(other_piece, other_piece, f_send.at[0], f_recv.at[5], on_chip).wait_recv()
     place_piece(corner)

time: 50.2 us -> 49.4 us (0.984)
  Pallas kernels: 49.5 us -> 48.6 us
    pallas_call x1, Pallas kernels: 47.4 us -> 46.5 us  [fused(): pl.pallas_call(layer_kernel, out_shape=(jax.ShapeDtypeStruct(first_batch....]
where the time goes in v4:
time: 49.4 us; the launch traced here: 49.2 us
  Pallas kernels  48.6 us (98%)
  between operations  0.64 us (1%)
    pallas_call x1, Pallas kernels, fused(): pl.pallas_call(layer_kernel, out_shape=(jax.ShapeDtypeStruct(first_batch....  46.5 us
    pallas_call x1, Pallas kernels, finish(): pl.pallas_call(finish_kernel, out_shape=tuple((jax.ShapeDtypeStruct(x.sha...  2.09 us

profile of v4, /device:TPU:1, one launch (start us, length us, event | category | flops | bytes accessed | tf_op | source)
XLA Modules:
  0.0 49.2 jit_solution(3016785592187165270)
XLA Ops:
  0.6 46.5 %layer.1 = (bf16[128,2048]{1,0:T(8,128)(2,1)}, bf16[128,2048]{1,0:T(8,128)(2,1)}) custom-call(bf16[128,2048]{1,0:T(8,128)(2,1)} %first_hbm.1, f32[1,2048]{1,0:T(1,128)} %bitcast.7, bf16[2048,128]{1,0:T(8,128)(2,1)} %mixer_in_hbm.1, bf16[512,64]{1,0:T(8,128)(2,1)} %bitcast.6, f32[1,512]{1,0:T(1,128)} %bitcast.9, bf16[128,2048]{1,0:T(8,128)(2,1)} %mixer_out_hbm.1, ...), custom_call_target="tpu_custom_call" | custom-call | flops 7000000000 | bytes 16777216 | tf_op jit(solution)/shard_map/layer/pallas_call | solution.py:665
  47.1 2.1 %finish.1 = (bf16[128,2048]{1,0:T(8,128)(2,1)}, bf16[128,2048]{1,0:T(8,128)(2,1)}) custom-call(bf16[128,2048]{1,0:T(8,128)(2,1)} %get-tuple-element.4.mixed, bf16[128,2048]{1,0:T(8,128)(2,1)} %get-tuple-element.5.result), custom_call_target="tpu_custom_call" | custom-call | tf_op jit(solution)/shard_map/finish/pallas_call | solution.py:630

commit v5 on v4

--- a/solution.py
+++ b/solution.py
@@ -536,7 +536,7 @@
     expert(2, 4, between=[lambda: turn(6)])
     spread_x(1)
     arrive(2)
-    expert(4, 6, [lambda: add_y(5, 2)], [lambda: turn(7), lambda: add_all(4)])
+    expert(4, 6, [lambda: add_y(5), lambda: add_all(4)], [lambda: turn(7), lambda: add_y(2)])
     arrive(3)
     expert(6, 8, [lambda: add_y(6)])
     add_all(5, 1)
@@ -606,19 +606,19 @@
 
 
 def finish_kernel(mixed, result, mixed_out, result_out, held, into, out):
-    step = held.shape[1] // 4
+    step = held.shape[1]
     loads, stores = [], []
     for i, source in enumerate((result, mixed)):
-        for j in range(4):
+        for j in range(1):
             rows = pl.ds(step * j, step)
-            copy = pltpu.make_async_copy(source.at[rows], held.at[i, rows], into.at[4 * i + j])
+            copy = pltpu.make_async_copy(source.at[rows], held.at[i, rows], into.at[i + j])
             copy.start()
             loads.append(copy)
     for i, target in enumerate((result_out, mixed_out)):
-        for j in range(4):
+        for j in range(1):
             rows = pl.ds(step * j, step)
-            loads[4 * i + j].wait()
-            copy = pltpu.make_async_copy(held.at[i, rows], target.at[rows], out.at[4 * i + j])
+            loads[i + j].wait()
+            copy = pltpu.make_async_copy(held.at[i, rows], target.at[rows], out.at[i + j])
             copy.start()
             stores.append(copy)
     for copy in stores:
@@ -634,8 +634,8 @@
         out_specs=(anywhere, anywhere),
         scratch_shapes=[
             pltpu.VMEM((2,) + result.shape, result.dtype),
-            pltpu.SemaphoreType.DMA((8,)),
-            pltpu.SemaphoreType.DMA((8,)),
+            pltpu.SemaphoreType.DMA((2,)),
+            pltpu.SemaphoreType.DMA((2,)),
         ],
         name="finish",
     )(mixed, result)

time: 49.4 us -> 49 us (level)
  Pallas kernels: 48.6 us -> 48.1 us
where the time goes in v5:
time: 49 us; the launch traced here: 48.8 us
  Pallas kernels  48.1 us (98%)
  between operations  0.64 us (1%)
    pallas_call x1, Pallas kernels, fused(): pl.pallas_call(layer_kernel, out_shape=(jax.ShapeDtypeStruct(first_batch....  46.1 us
    pallas_call x1, Pallas kernels, finish(): pl.pallas_call(finish_kernel, out_shape=tuple((jax.ShapeDtypeStruct(x.sha...  2.04 us

profile of v5, /device:TPU:1, one launch (start us, length us, event | category | flops | bytes accessed | tf_op | source)
XLA Modules:
  0.0 48.8 jit_solution(15250070225860263177)
XLA Ops:
  0.6 46.1 %layer.1 = (bf16[128,2048]{1,0:T(8,128)(2,1)}, bf16[128,2048]{1,0:T(8,128)(2,1)}) custom-call(bf16[128,2048]{1,0:T(8,128)(2,1)} %first_hbm.1, f32[1,2048]{1,0:T(1,128)} %bitcast.7, bf16[2048,128]{1,0:T(8,128)(2,1)} %mixer_in_hbm.1, bf16[512,64]{1,0:T(8,128)(2,1)} %bitcast.6, f32[1,512]{1,0:T(1,128)} %bitcast.9, bf16[128,2048]{1,0:T(8,128)(2,1)} %mixer_out_hbm.1, ...), custom_call_target="tpu_custom_call" | custom-call | flops 7000000000 | bytes 16777216 | tf_op jit(solution)/shard_map/layer/pallas_call | solution.py:665
  46.8 2.0 %finish.1 = (bf16[128,2048]{1,0:T(8,128)(2,1)}, bf16[128,2048]{1,0:T(8,128)(2,1)}) custom-call(bf16[128,2048]{1,0:T(8,128)(2,1)} %get-tuple-element.4.mixed, bf16[128,2048]{1,0:T(8,128)(2,1)} %get-tuple-element.5.result), custom_call_target="tpu_custom_call" | custom-call | tf_op jit(solution)/shard_map/finish/pallas_call | solution.py:630
